TPU v7x, 512 devices: a whole 4x4x16 slice. The times are simulated.
512 devices in a mesh: ep: 128 (over z, x, core), tp: 4 (over y).
Axes of the slice: x: 4, y: 4, z: 16, core: 2. Of those that a mesh axis runs over, the one named last changes fastest.
Arguments:
- tokens: bfloat16 [512, 2048], P('ep'), may hold values from -6 to 6
- norm_gain: bfloat16 [2048], replicated, may hold values from 0.099609375 to 1.8984375
- in_weight: bfloat16 [2048, 1024], P(None, 'tp'), may hold values from -0.125 to 0.125
- decay_rate: float32 [64, 64], P('tp'), may hold values from 0.05 to 1
- frequency: float32 [64, 64], P('tp'), may hold values from -3 to 3
- log_step: float32 [64], P('tp'), may hold values from -2.3 to 0.7
- input_real: float32 [64, 64, 16], P('tp'), may hold values from -1.75 to 1.75
- input_imag: float32 [64, 64, 16], P('tp'), may hold values from -1.75 to 1.75
- output_real: float32 [64, 16, 64], P('tp'), may hold values from -0.5 to 0.5
- output_imag: float32 [64, 16, 64], P('tp'), may hold values from -0.5 to 0.5
- skip_gain: float32 [1024], P('tp'), may hold values from -3 to 3
- state_real: float32 [512, 64, 64], P('ep', 'tp'), may hold values from -6 to 6
- state_imag: float32 [512, 64, 64], P('ep', 'tp'), may hold values from -6 to 6
- out_weight: bfloat16 [1024, 2048], P('tp'), may hold values from -0.1875 to 0.1875
- ffn_gain: bfloat16 [2048], replicated, may hold values from 0.099609375 to 1.8984375
- expert_ids: int32 [512, 2], replicated, may hold values from 0 to 7, all different within a row; in each aligned block of 4 rows (0 to 3, 4 to 7, ...) at most 2 rows name the same one
- route_weights: float32 [512, 2], P('ep'), may hold values from 0.2 to 1
- gate_weight: bfloat16 [2048, 65536], P(None, ('ep', 'tp')), may hold values from -0.125 to 0.125
- up_weight: bfloat16 [2048, 65536], P(None, ('ep', 'tp')), may hold values from -0.125 to 0.125
- down_weight: bfloat16 [65536, 2048], P('ep', 'tp'), may hold values from -0.0625 to 0.0625
Outputs:
- mixed: bfloat16 [512, 2048], P('ep', 'tp')
- new_real: float32 [512, 64, 64], P('ep', 'tp')
- new_imag: float32 [512, 64, 64], P('ep', 'tp')
Inputs may be any that keep to these rules, and one draw needn't show every extreme that they name: `expert_ids`: the 2 experts of a row differ. In each aligned block of 4 rows (the rows of one index of ep) no expert is named by more than 2 rows, and in some blocks one expert is named by exactly 2 rows.
All inputs are finite; a program needn't handle non-finite values.
Results may differ from a plain program's by a relative error of at most 0.007.
Values may be sent and summed in bfloat16 or wider, within the bound.
A program may use at most 64 MiB of HBM per device.

v0:
```python
import jax
import jax.numpy as jnp
from jax import lax
from jax.sharding import PartitionSpec as P

EXPERTS = 8


EPSILON = 1e-06


def sent_to_all(x, axis):
    length = lax.axis_size(axis)
    return lax.all_to_all(jnp.broadcast_to(x[None], (length, *x.shape)), axis, 0, 0, tiled=True)


def over_copies(x, axis):
    return sent_to_all(x, axis).sum(axis=0)


def joined_along(tiles, dim):
    tiles = jnp.moveaxis(tiles, 0, dim)
    lengths = tiles.shape
    return tiles.reshape(*lengths[:dim], lengths[dim] * lengths[dim + 1], *lengths[dim + 2 :])


def gather_directly(x, axis, dim):
    tiles = sent_to_all(x, axis)
    return joined_along(tiles, dim)


def rms_scale(values, gain):
    floats = values.astype(jnp.float32)
    return (
        floats
        * lax.rsqrt(jnp.mean(floats * floats, axis=-1, keepdims=True) + EPSILON)
        * gain.astype(jnp.float32)
    )


def discretize(decay_rate, frequency, log_step, input_real, input_imag):
    step_size = jnp.exp(log_step)[:, None]
    lam_real = -decay_rate
    magnitude = jnp.exp(lam_real * step_size)
    turned = frequency * step_size
    bar_real = magnitude * jnp.cos(turned)
    bar_imag = magnitude * jnp.sin(turned)
    denom = lam_real * lam_real + frequency * frequency
    minus_one = bar_real - 1.0
    factor_real = (minus_one * lam_real + bar_imag * frequency) / denom
    factor_imag = (bar_imag * lam_real - minus_one * frequency) / denom
    b_real = factor_real[..., None] * input_real - factor_imag[..., None] * input_imag
    b_imag = factor_real[..., None] * input_imag + factor_imag[..., None] * input_real
    return (bar_real, bar_imag, b_real, b_imag)


def state_update(
    projected,
    state_real,
    state_imag,
    decay_rate,
    frequency,
    log_step,
    input_real,
    input_imag,
    output_real,
    output_imag,
    skip_gain,
):
    bar_real, bar_imag, b_real, b_imag = discretize(
        decay_rate, frequency, log_step, input_real, input_imag
    )
    count, groups, _ = state_real.shape
    high = lax.Precision.HIGHEST
    grouped = projected.astype(jnp.float32).reshape(count, groups, -1)
    drive_real = jnp.einsum("sgp,gnp->sgn", grouped, b_real, precision=high)
    drive_imag = jnp.einsum("sgp,gnp->sgn", grouped, b_imag, precision=high)
    new_real = bar_real * state_real - bar_imag * state_imag + drive_real
    new_imag = bar_real * state_imag + bar_imag * state_real + drive_imag
    readout = jnp.einsum("sgn,gpn->sgp", new_real, output_real, precision=high) - jnp.einsum(
        "sgn,gpn->sgp", new_imag, output_imag, precision=high
    )
    readout = readout.reshape(count, -1) + skip_gain * grouped.reshape(count, -1)
    return (jax.nn.gelu(readout).astype(jnp.bfloat16), new_real, new_imag)


def slot_table(own_ids, own_weights, slot_count):
    expert_range = jnp.arange(EXPERTS, dtype=jnp.int32)
    onehot = (own_ids[:, :, None] == expert_range).astype(jnp.int32)
    flat = onehot.reshape(-1, EXPERTS)
    before = (jnp.cumsum(flat, axis=0) - flat).reshape(onehot.shape)
    slots = jnp.arange(slot_count, dtype=jnp.int32)
    match = (before[..., None] == slots) & (onehot[..., None] > 0)
    table = jnp.sum(jnp.where(match, own_weights[:, :, None, None], 0.0), axis=1)
    return jnp.transpose(table, (1, 2, 0))


def shards(
    tokens,
    norm_gain,
    in_weight,
    decay_rate,
    frequency,
    log_step,
    input_real,
    input_imag,
    output_real,
    output_imag,
    skip_gain,
    state_real,
    state_imag,
    out_weight,
    ffn_gain,
    expert_ids,
    route_weights,
    gate_weight,
    up_weight,
    down_weight,
):
    normed_in = rms_scale(tokens, norm_gain).astype(jnp.bfloat16)
    projected = jnp.dot(normed_in, in_weight, preferred_element_type=jnp.float32).astype(
        jnp.bfloat16
    )
    activated, new_real, new_imag = state_update(
        projected,
        state_real,
        state_imag,
        decay_rate,
        frequency,
        log_step,
        input_real,
        input_imag,
        output_real,
        output_imag,
        skip_gain,
    )
    delta = over_copies(jnp.dot(activated, out_weight, preferred_element_type=jnp.float32), "tp")
    hidden_state = (tokens.astype(jnp.float32) + delta).astype(jnp.bfloat16)
    normed = rms_scale(hidden_state, ffn_gain).astype(jnp.bfloat16)
    seq_count, width = normed.shape
    slot_count = seq_count // 2
    group_span = lax.axis_size("ep") // EXPERTS
    my_index = lax.axis_index("ep")
    own_ids = lax.dynamic_slice_in_dim(expert_ids, my_index * seq_count, seq_count, 0)
    unit_weights = jnp.ones(own_ids.shape, jnp.float32)
    select = slot_table(own_ids, unit_weights, slot_count)
    outgoing = jnp.einsum(
        "xcs,sd->xcd", select.astype(jnp.bfloat16), normed, preferred_element_type=jnp.float32
    ).astype(jnp.bfloat16)
    received = lax.all_to_all(
        jnp.repeat(outgoing, group_span, axis=0), "ep", split_axis=0, concat_axis=0, tiled=True
    )
    slot_rows = received.reshape(-1, width)
    gate_pre = jnp.dot(slot_rows, gate_weight, preferred_element_type=jnp.float32)
    up_pre = jnp.dot(slot_rows, up_weight, preferred_element_type=jnp.float32)
    hidden = (jax.nn.silu(gate_pre) * up_pre).astype(jnp.bfloat16)
    quarter = down_weight.shape[1]
    partial_out = jnp.dot(
        gather_directly(hidden, "tp", 1), down_weight, preferred_element_type=jnp.float32
    )
    rounded = partial_out.astype(jnp.bfloat16).reshape(-1, slot_count, quarter)
    returned = lax.all_to_all(rounded, "ep", split_axis=0, concat_axis=0, tiled=True)
    summed = (
        returned.astype(jnp.float32).reshape(EXPERTS, group_span, slot_count, quarter).sum(axis=1)
    )
    weight_table = slot_table(own_ids, route_weights, slot_count)
    routed = jnp.einsum("xcs,xcd->sd", weight_table, summed, precision=lax.Precision.HIGHEST)
    residual = lax.dynamic_slice_in_dim(hidden_state, lax.axis_index("tp") * quarter, quarter, 1)
    mixed = (residual.astype(jnp.float32) + routed).astype(jnp.bfloat16)
    return (mixed, new_real, new_imag)


def solution(mesh):
    in_specs = (
        P("ep", None),
        P(),
        P(None, "tp"),
        P("tp", None),
        P("tp", None),
        P("tp"),
        P("tp", None, None),
        P("tp", None, None),
        P("tp", None, None),
        P("tp", None, None),
        P("tp"),
        P("ep", "tp", None),
        P("ep", "tp", None),
        P("tp", None),
        P(),
        P(),
        P("ep", None),
        P(None, ("ep", "tp")),
        P(None, ("ep", "tp")),
        P("ep", "tp"),
    )
    out_specs = (P("ep", "tp"), P("ep", "tp", None), P("ep", "tp", None))
    return jax.shard_map(shards, mesh=mesh, in_specs=in_specs, out_specs=out_specs, check_vma=False)
```

profile of v0, /device:TPU:1, one launch (start us, length us, event | category | flops | bytes accessed | tf_op | source)
XLA Modules:
  0.0 137.2 jit_solution(15383408067632436841)
XLA Ops:
  0.6 0.0 copy-start
  0.7 0.8 exp.10
  1.4 0.9 fusion.19
  2.4 1.5 %convolution_convert_fusion.2 = bf16[4,256]{1,0:T(4,128)(2,1)S(1)} fusion(bf16[2048,256]{1,0:T(8,128)(2,1)} %param.22, bf16[4,2048]{1,0:T(4,128)(2,1)S(1)} %copy-done.4, f32[2048]{0:T(1024)S(1)} %convert_element_type.68, f32[4]{0:T(128)S(1)} %add_rsqrt_fusion.1), kind=kOutput, calls=%fused_computation.13 | convolution fusion | flops 4228096 | bytes 1075216 | tf_op jit(solution)/shard_map/dot_general | solution.py:121
  3.9 0.1 reshape.83
  4.0 0.0 copy-done.9
  4.0 0.1 cosine_multiply_fusion
  4.2 0.5 copy-done.6
  4.7 0.1 copy-done.5
  4.8 0.2 fusion.2
  5.0 0.2 fusion.3
  5.2 0.7 copy-done.8
  5.9 0.3 fusion.60
  6.2 0.6 copy-done.7
  6.8 0.3 fusion.1
  7.2 0.1 reshape.84
  7.2 0.6 copy-done.13
  7.8 0.2 fusion.46
  8.1 0.7 broadcast_in_dim.20
  8.7 5.0 %all-to-all-start = ((f32[4,4,2048]{2,1,0:T(4,128)}), f32[4,4,2048]{2,1,0:T(4,128)S(1)}, u32[]{:S(2)}, u32[]{:S(2)}) async-start(f32[4,4,2048]{2,1,0:T(4,128)} %broadcast_in_dim.20), calls=%async_computation | async-start | bytes 262144 | tf_op jit(solution)/shard_map/all_to_all | solution.py:14
  13.7 0.7 constant_dynamic-slice_fusion
  14.5 0.1 copy.72
  14.6 0.1 eq.56
  14.7 0.1 fusion.42
  14.8 0.1 fusion.45
  14.9 0.1 fusion.43
  14.9 0.7 copy-done.12
  15.6 0.7 copy-done.14
  16.3 0.1 select_reduce_fusion.1
  16.4 2.2 %all-to-all-done = f32[4,4,2048]{2,1,0:T(4,128)S(1)} async-done(((f32[4,4,2048]{2,1,0:T(4,128)}), f32[4,4,2048]{2,1,0:T(4,128)S(1)}, u32[]{:S(2)}, u32[]{:S(2)}) %all-to-all-start) | async-done | bytes 131104 | tf_op jit(solution)/shard_map/all_to_all | solution.py:14
  18.6 0.1 fusion.16
  18.7 0.2 convolution_convert_fusion
  19.0 0.1 copy.76
  19.0 0.6 broadcast_in_dim.24
  19.7 72.9 %all_to_all.20 = bf16[128,2,2048]{2,1,0:T(2,128)(2,1)S(1)} all-to-all(bf16[128,2,2048]{2,1,0:T(2,128)(2,1)S(1)} %bitcast.45), channel_id=1, replica_groups=mesh['ep'=128,'tp'=4] {'ep'}, dimensions={0} | all-to-all | bytes 2097152 | tf_op jit(solution)/shard_map/all_to_all | solution.py:150
  92.6 0.4 reshape.86
  93.0 1.5 %fusion.61 = f32[256,128]{1,0:T(8,128)S(1)} fusion(bf16[256,2048]{1,0:T(8,128)(2,1)S(1)} %reshape.86, bf16[2048,128]{1,0:T(8,128)(2,1)} %param.37), kind=kOutput, calls=%fused_computation.86 | convolution fusion | flops 134217728 | bytes 1703936 | tf_op jit(solution)/shard_map/dot_general | solution.py:154
  94.5 0.4 fusion
  95.0 0.1 copy.77
  95.1 7.9 %all_to_all.21 = bf16[4,256,128]{1,2,0:T(8,128)(2,1)S(1)} all-to-all(bf16[4,256,128]{1,2,0:T(8,128)(2,1)S(1)} %broadcast_in_dim.25), channel_id=1, replica_groups=mesh['ep'=128,'tp'=4] {'tp'}, dimensions={0} | all-to-all | bytes 524288 | tf_op jit(solution)/shard_map/all_to_all | solution.py:14
  103.0 0.3 convolution_convert_fusion.1
  103.4 0.8 reshape.88
  104.1 11.6 %all-to-all-start.3 = ((bf16[128,2,512]{2,1,0:T(2,128)(2,1)}), bf16[128,2,512]{2,1,0:T(2,128)(2,1)S(1)}, u32[]{:S(2)}, u32[]{:S(2)}) async-start(bf16[128,2,512]{2,1,0:T(2,128)(2,1)} %reshape.88), calls=%async_computation.3 | async-start | bytes 524288 | tf_op jit(solution)/shard_map/all_to_all | solution.py:162
  115.8 0.6 copy.79
  116.4 0.6 copy.80
  117.0 19.2 %all-to-all-done.3 = bf16[128,2,512]{2,1,0:T(2,128)(2,1)S(1)} async-done(((bf16[128,2,512]{2,1,0:T(2,128)(2,1)}), bf16[128,2,512]{2,1,0:T(2,128)(2,1)S(1)}, u32[]{:S(2)}, u32[]{:S(2)}) %all-to-all-start.3) | async-done | bytes 262176 | tf_op jit(solution)/shard_map/all_to_all | solution.py:162
  136.2 0.2 convert_reduce_fusion
  136.4 0.8 fusion.5
  (33 shorter events, 0.2 us)
Async XLA Ops:
  0.6 6.6 %copy-start = (bf16[256,2048]{1,0:T(8,128)(2,1)S(1)}, bf16[256,2048]{1,0:T(8,128)(2,1)}, u32[]{:S(2)}) copy-start(bf16[256,2048]{1,0:T(8,128)(2,1)} %param.33) | copy-start | bytes 3145732
  0.6 1.7 %copy-start.4 = (bf16[4,2048]{1,0:T(4,128)(2,1)S(1)}, bf16[4,2048]{1,0:T(4,128)(2,1)}, u32[]{:S(2)}) copy-start(bf16[4,2048]{1,0:T(4,128)(2,1)} %param.20) | copy-start | bytes 49156
  1.4 0.9 copy-start.11
  2.3 1.7 %copy-start.9 = (f32[16,64]{1,0:T(8,128)S(1)}, f32[16,64]{1,0:T(8,128)}, u32[]{:S(2)}) copy-start(f32[16,64]{1,0:T(8,128)} %param.24) | copy-start | bytes 12292
  2.3 1.7 %copy-start.10 = (f32[16,64]{1,0:T(8,128)S(1)}, f32[16,64]{1,0:T(8,128)}, u32[]{:S(2)}) copy-start(f32[16,64]{1,0:T(8,128)} %param.23) | copy-start | bytes 12292
  2.3 1.8 %copy-start.1 = (f32[16,64,16]{1,2,0:T(8,128)S(1)}, f32[16,64,16]{1,2,0:T(8,128)}, u32[]{:S(2)}) copy-start(f32[16,64,16]{1,2,0:T(8,128)} %param.27) | copy-start | bytes 196612
  2.3 1.8 %copy-start.2 = (f32[16,64,16]{1,2,0:T(8,128)S(1)}, f32[16,64,16]{1,2,0:T(8,128)}, u32[]{:S(2)}) copy-start(f32[16,64,16]{1,2,0:T(8,128)} %param.26) | copy-start | bytes 196612
  3.9 0.8 copy-start.6
  4.0 0.8 copy-start.5
  5.0 0.9 copy-start.8
  5.9 0.9 copy-start.7
  7.1 0.7 copy-start.13
  8.7 9.8 %all-to-all-start = ((f32[4,4,2048]{2,1,0:T(4,128)}), f32[4,4,2048]{2,1,0:T(4,128)S(1)}, u32[]{:S(2)}, u32[]{:S(2)}) async-start(f32[4,4,2048]{2,1,0:T(4,128)} %broadcast_in_dim.20), calls=%async_computation | async-start | bytes 262144 | tf_op jit(solution)/shard_map/all_to_all | solution.py:14
  14.9 0.7 copy-start.12
  15.6 0.7 copy-start.14
  93.0 1.5 %copy-start.15 = (bf16[2048,128]{1,0:T(8,128)(2,1)S(1)}, bf16[2048,128]{1,0:T(8,128)(2,1)}, u32[]{:S(2)}) copy-start(bf16[2048,128]{1,0:T(8,128)(2,1)} %param.38) | copy-start | bytes 1572868
  95.0 8.1 %copy-start.3 = (bf16[512,512]{1,0:T(8,128)(2,1)S(1)}, bf16[512,512]{1,0:T(8,128)(2,1)}, u32[]{:S(2)}) copy-start(bf16[512,512]{1,0:T(8,128)(2,1)} %param.39) | copy-start | bytes 1572868
  104.1 32.0 %all-to-all-start.3 = ((bf16[128,2,512]{2,1,0:T(2,128)(2,1)}), bf16[128,2,512]{2,1,0:T(2,128)(2,1)S(1)}, u32[]{:S(2)}, u32[]{:S(2)}) async-start(bf16[128,2,512]{2,1,0:T(2,128)(2,1)} %reshape.88), calls=%async_computation.3 | async-start | bytes 524288 | tf_op jit(solution)/shard_map/all_to_all | solution.py:162
where the time goes:
time: 139 us; the launch traced here: 137 us
  blocking collectives  80.8 us (58%)
  waiting for transfers between devices  21.4 us (15%)
  starting transfers between devices  16.6 us (12%)
  local copies, waits for them, and re-layouts  9.71 us (7%)
  matrix products  6.13 us (4%)
  other arithmetic  1.71 us (1%)
    all_to_all x1, blocking collectives, shards(): lax.all_to_all(jnp.repeat(outgoing, group_span, axis=0), 'ep', split_axis...  72.9 us
    all_to_all x1, waiting for transfers between devices, shards(): lax.all_to_all(rounded, 'ep', split_axis=0, concat_axis=0, tiled=True)  19.2 us
    all_to_all x1, starting transfers between devices, shards(): lax.all_to_all(rounded, 'ep', split_axis=0, concat_axis=0, tiled=True)  11.6 us
    all_to_all x1, blocking collectives, sent_to_all(): lax.all_to_all(jnp.broadcast_to(x[None], (length, *x.shape)), axis, 0, 0,...  7.92 us
    unnamed x34, local copies, waits for them, and re-layouts  5.13 us
    all_to_all x1, starting transfers between devices, sent_to_all(): lax.all_to_all(jnp.broadcast_to(x[None], (length, *x.shape)), axis, 0, 0,...  5 us
  transfers between devices with their start and end apart: 2, of which 2 were waited for; matrix products, arithmetic and copies ran while one was open for 2% of the time, Pallas kernels for 0%

commit v1 on v0

v1 whole, which is shorter than its diff:
```python
import jax
import jax.numpy as jnp
from jax import lax
from jax.experimental import pallas as pl
from jax.experimental.pallas import tpu as pltpu
from jax.sharding import PartitionSpec as P

EPS = 1e-06
F32, BF16, I32 = jnp.float32, jnp.bfloat16, jnp.int32
MESH = pl.DeviceIdType.MESH
NX, NY, NC, NZ = 4, 4, 2, 16
SEQ, WIDTH, QUARTER = 4, 2048, 512
GROUPS, STATE, CHANNELS = 16, 64, 256
HID = 128
CHUNKS = ((0, 1, 15, 2, 14, 3, 13, 4), (12, 5, 11, 6, 10, 7, 9, 8))
PLANE = sorted(
    [(dx, dy) for dx in range(NX) for dy in range(NY)],
    key=lambda d: min(d[0], NX - d[0]) + min(d[1], NY - d[1]),
)


def iota(shape, dim):
    return lax.broadcasted_iota(I32, shape, dim)


def dot(a, b):
    return jnp.dot(a, b, preferred_element_type=F32)


def dot_t(a, b):
    return lax.dot_general(a, b, (((1,), (1,)), ((), ())), preferred_element_type=F32)


def split(x):
    high = x.astype(BF16)
    return high, (x - high.astype(F32)).astype(BF16)


def row_of(block):
    block = block.astype(F32)
    return jnp.concatenate([block[i : i + 1, :] for i in range(block.shape[0])], axis=1)


def rms(floats, gain):
    scale = lax.rsqrt(jnp.mean(floats * floats, axis=-1, keepdims=True) + EPS)
    return (floats * scale * gain).astype(BF16)


def kernel(*refs):
    hbm, outs, scratch = refs[:20], refs[20:23], refs[23:]
    (tok_h, gain_h, inw_h, decay_h, freq_h, step_h, inr_h, ini_h, outr_h, outi_h) = hbm[:10]
    (skip_h, str_h, sti_h, outw_h, fgain_h, ids_h, rw_h, gw_h, uw_h, dw_h) = hbm[10:]
    mixed_o, newr_o, newi_o = outs
    (tok, gain, inw, decay, freq, steps, inr, ini, outr, outi) = scratch[:10]
    (skip, st_r, st_i, outw, fgain, ids, rw, gw, uw, dw) = scratch[10:20]
    (newr, newi, mixed, delta, norm32, hid32, pick32, pick, zin) = scratch[20:29]
    (gat, hid, send, recv, sum32, back, zout, load, store) = scratch[29:38]
    (ds_sem, dr_sem, zs_sem, zr_sem, gs_sem, gr_sem, fs_sem, fr_sem) = scratch[38:46]
    (hs_sem, hr_sem, rs_sem, rr_sem, bs_sem, br_sem) = scratch[46:52]

    ep, y = lax.axis_index("ep"), lax.axis_index("tp")
    z, x, c = ep // 8, (ep // 2) % NX, ep % 2

    def at(zz, xx, cc, yy):
        return (zz * 8 + xx * 2 + cc, yy)

    def turn(a, d, n):
        return lax.rem(a + d, n)

    barrier = pltpu.get_barrier_semaphore()
    partners = [at(turn(z, d, NZ), x, c, y) for d in range(1, NZ)]
    partners += [at(z, turn(x, dx, NX), c, turn(y, dy, NY)) for dx, dy in PLANE if dx or dy]
    partners += [at(z, turn(x, dx, NX), 1 - c, y) for dx in range(NX)]
    for device in partners:
        pl.semaphore_signal(barrier, inc=1, device_id=device, device_id_type=MESH)

    wide = pl.multiple_of((ep // 32) * 128, 128)
    sources = list(hbm)
    sources[15] = ids_h.at[:, pl.ds(wide, 128)]
    loads = [
        pltpu.make_async_copy(source, target, load.at[i])
        for i, (source, target) in enumerate(zip(sources, scratch[:20]))
    ]
    for i in (0, 1, 2, 3, 4, 5, 6, 7, 11, 12, 8, 9, 10, 13, 14, 15, 16, 17, 18, 19):
        loads[i].start()

    loads[0].wait()
    loads[1].wait()
    tokens = tok[...].astype(F32)
    normed_in = rms(tokens, row_of(gain[...]))
    loads[2].wait()
    u = dot(normed_in, inw[...]).astype(BF16).astype(F32)

    rows = SEQ * GROUPS
    own_group = iota((rows, CHANNELS), 0) % GROUPS == iota((rows, CHANNELS), 1) // 16
    spread = jnp.broadcast_to(u[:, None, :], (SEQ, GROUPS, CHANNELS)).reshape(rows, CHANNELS)
    spread = jnp.where(own_group, spread, 0.0).astype(BF16)
    for i in (3, 4, 5, 6, 7):
        loads[i].wait()
    group_row = iota((GROUPS, STATE), 0)
    log_step = jnp.zeros((GROUPS, STATE), F32)
    for g in range(GROUPS):
        log_step = jnp.where(group_row == g, steps[g], log_step)
    step_size = jnp.exp(log_step)
    lam_real, frequency = -decay[...], freq[...]
    magnitude = jnp.exp(lam_real * step_size)
    turned = frequency * step_size
    bar_real = magnitude * jnp.cos(turned)
    bar_imag = magnitude * jnp.sin(turned)
    denom = lam_real * lam_real + frequency * frequency
    minus_one = bar_real - 1.0
    factor_real = (minus_one * lam_real + bar_imag * frequency) / denom
    factor_imag = (bar_imag * lam_real - minus_one * frequency) / denom

    def per_row(v):
        return jnp.broadcast_to(v[None], (SEQ, GROUPS, STATE)).reshape(rows, STATE)

    def drive(ref):
        high, low = split(ref[...].reshape(CHANNELS, STATE))
        return dot(spread, high) + dot(spread, low)

    drive_r, drive_i = drive(inr), drive(ini)
    bar_real, bar_imag = per_row(bar_real), per_row(bar_imag)
    factor_real, factor_imag = per_row(factor_real), per_row(factor_imag)
    loads[11].wait()
    loads[12].wait()
    state_r, state_i = st_r[...].reshape(rows, STATE), st_i[...].reshape(rows, STATE)
    new_r = (bar_real * state_r - bar_imag * state_i) + (factor_real * drive_r - factor_imag * drive_i)
    new_i = (bar_real * state_i + bar_imag * state_r) + (factor_real * drive_i + factor_imag * drive_r)
    newr[...] = new_r.reshape(SEQ, GROUPS, STATE)
    newi[...] = new_i.reshape(SEQ, GROUPS, STATE)

    for i in (8, 9, 10):
        loads[i].wait()

    def read(values, ref):
        high, low = split(values)
        ref_high, ref_low = split(ref[...].reshape(CHANNELS, STATE))
        return dot_t(high, ref_high) + dot_t(high, ref_low) + dot_t(low, ref_high)

    readout = jnp.where(own_group, read(new_r, outr) - read(new_i, outi), 0.0)
    readout = readout.reshape(SEQ, GROUPS, CHANNELS).sum(axis=1)
    readout = readout + row_of(skip[...]) * u
    activated = jax.nn.gelu(readout).astype(BF16)
    loads[13].wait()
    delta[y] = dot(activated, outw[...]).astype(BF16)

    pl.semaphore_wait(barrier, len(partners))
    delta_copies = [
        pltpu.make_async_remote_copy(
            delta.at[y], delta.at[y], ds_sem.at[d], dr_sem.at[d],
            device_id=at(z, x, c, turn(y, d, NY)), device_id_type=MESH,
        )
        for d in range(1, NY)
    ]
    for copy in delta_copies:
        copy.start()
    stores = [
        pltpu.make_async_copy(newr, newr_o, store.at[0]),
        pltpu.make_async_copy(newi, newi_o, store.at[1]),
    ]
    for copy in stores:
        copy.start()

    for i in (14, 15, 16):
        loads[i].wait()
    first = (ep % 32) * SEQ
    names = [[ids[k, first + s] for k in range(2)] for s in range(SEQ)]
    weights = [[rw[k, s] for k in range(2)] for s in range(SEQ)]

    def table(expert, slot, shape):
        taken = jnp.zeros(shape, I32)
        picks, scales = [], []
        for s in range(SEQ):
            routes = [expert == names[s][k] for k in range(2)]
            named = routes[0] | routes[1]
            here = named & (taken == slot)
            picks.append(jnp.where(here, 1.0, 0.0))
            scale = jnp.where(routes[0], weights[s][0], 0.0) + jnp.where(routes[1], weights[s][1], 0.0)
            scales.append(jnp.where(here, scale, 0.0))
            taken = taken + jnp.where(named, 1, 0)
        return picks, scales

    pick_row = iota((16, QUARTER), 0)
    picks, _ = table(pick_row // 2, pick_row % 2, (16, QUARTER))
    ffn_gain = row_of(fgain[...])

    for copy in delta_copies:
        copy.wait_recv()
    total = tokens
    for i in range(NY):
        total = total + delta[i].astype(F32)
    hidden_state = total.astype(BF16).astype(F32)
    hid32[...] = hidden_state
    norm32[...] = rms(hidden_state, ffn_gain).astype(F32)
    lanes = pl.ds(pl.multiple_of(y * QUARTER, QUARTER), QUARTER)
    own = norm32[:, lanes]
    chosen = picks[0] * own[0:1, :]
    for s in range(1, SEQ):
        chosen = chosen + picks[s] * own[s : s + 1, :]
    pick32[...] = chosen
    for e in range(8):
        pick[e] = pick32[2 * e : 2 * e + 2, :].astype(BF16)

    z_copies = {}
    for d in (8, 7, 9, 6, 10, 5, 11, 4, 12, 3, 13, 2, 14, 1, 15):
        to = turn(z, d, NZ)
        z_copies[d] = pltpu.make_async_remote_copy(
            pick.at[to // 2], zin.at[d], zs_sem.at[d], zr_sem.at[d],
            device_id=at(to, x, c, y), device_id_type=MESH,
        )
        z_copies[d].start()

    gathers, forwards = [], []
    for k, chunk in enumerate(CHUNKS):
        for i, d in enumerate(chunk):
            if d:
                z_copies[d].wait_recv()
                piece = zin[d]
            else:
                piece = pick[z // 2]
            sum32[2 * i : 2 * i + 2, :] = piece.astype(F32)
        gat[k, y, c, x] = sum32[...].astype(BF16)
        copies = {}
        for dx, dy in reversed(PLANE):
            if dx or dy:
                copies[dx, dy] = pltpu.make_async_remote_copy(
                    gat.at[k, y, c, x], gat.at[k, y, c, x], gs_sem.at[k, dx, dy], gr_sem.at[k, dx, dy],
                    device_id=at(z, turn(x, dx, NX), c, turn(y, dy, NY)), device_id_type=MESH,
                )
                copies[dx, dy].start()
        gathers.append(copies)

    h_copies, r_copies = [], []

    def spread_chunk(k):
        copies = []
        for dx, dy in PLANE:
            if dx or dy:
                gathers[k][dx, dy].wait_recv()
            slot = gat.at[k, turn(y, NY - dy, NY), c, turn(x, NX - dx, NX)]
            copies.append(
                pltpu.make_async_remote_copy(
                    slot, slot, fs_sem.at[k, dx, dy], fr_sem.at[k, dx, dy],
                    device_id=at(z, x, 1 - c, y), device_id_type=MESH,
                )
            )
            copies[-1].start()
        forwards.append(copies)

    def up_chunk(k):
        for copy in forwards[k]:
            copy.wait_recv()
        gate_pre = jnp.zeros((128, HID), F32)
        up_pre = jnp.zeros((128, HID), F32)
        for q in range(NY):
            block = gat[k, q].reshape(128, QUARTER)
            gate_pre = gate_pre + dot(block, gw[q * QUARTER : (q + 1) * QUARTER, :])
            up_pre = up_pre + dot(block, uw[q * QUARTER : (q + 1) * QUARTER, :])
        units = pl.ds(pl.multiple_of(y * HID, HID), HID)
        hid[k, :, units] = (jax.nn.silu(gate_pre) * up_pre).astype(BF16)
        copies = []
        for d in (2, 1, 3):
            copies.append(
                pltpu.make_async_remote_copy(
                    hid.at[k, :, units], hid.at[k, :, units], hs_sem.at[k, d], hr_sem.at[k, d],
                    device_id=at(z, x, c, turn(y, d, NY)), device_id_type=MESH,
                )
            )
            copies[-1].start()
        h_copies.append(copies)

    def down_chunk(k):
        for copy in h_copies[k]:
            copy.wait_recv()
        send[k] = dot(hid[k], dw[...]).astype(BF16).reshape(NC, NX, 16, QUARTER)
        copies = []
        for dx in (2, 1, 3, 0):
            for dc in range(NC):
                if dx or dc:
                    to_x, to_c = turn(x, dx, NX), c if dc == 0 else 1 - c
                    copies.append(
                        pltpu.make_async_remote_copy(
                            send.at[k, to_c, to_x], recv.at[k, dc, dx], rs_sem.at[k, dc, dx], rr_sem.at[k, dc, dx],
                            device_id=at(z, to_x, to_c, y), device_id_type=MESH,
                        )
                    )
                    copies[-1].start()
        r_copies.append(copies)

    b_copies = {}

    def home_chunk(k):
        for copy in r_copies[k]:
            copy.wait_recv()
        total = send[k, c, x].astype(F32)
        for dc in range(NC):
            for dx in range(NX):
                if dx or dc:
                    total = total + recv[k, dc, dx].astype(F32)
        sum32[...] = total
        for i, d in enumerate(CHUNKS[k]):
            back[k, i] = sum32[2 * i : 2 * i + 2, :].astype(BF16)
        for i, d in reversed(list(enumerate(CHUNKS[k]))):
            if d:
                b_copies[d] = pltpu.make_async_remote_copy(
                    back.at[k, i], zout.at[d], bs_sem.at[d], br_sem.at[d],
                    device_id=at(turn(z, NZ - d, NZ), x, c, y), device_id_type=MESH,
                )
                b_copies[d].start()

    spread_chunk(0)
    loads[17].wait()
    loads[18].wait()
    up_chunk(0)
    spread_chunk(1)
    loads[19].wait()
    down_chunk(0)
    up_chunk(1)
    down_chunk(1)
    home_chunk(0)
    home_chunk(1)

    back_row = iota((2 * NZ, QUARTER), 0)
    _, scales = table(((z + back_row // 2) % NZ) // 2, back_row % 2, (2 * NZ, QUARTER))
    out32, mix32 = scratch[52], scratch[53]
    for d in (0, 1, 15, 2, 14, 3, 13, 4, 12, 5, 11, 6, 10, 7, 9, 8):
        if d:
            b_copies[d].wait_recv()
            piece = zout[d]
        else:
            piece = back[0, 0]
        out32[2 * d : 2 * d + 2, :] = piece.astype(F32)
    pieces = out32[...]
    for s in range(SEQ):
        mix32[s : s + 1, :] = jnp.sum(scales[s] * pieces, axis=0, keepdims=True)
    mixed[...] = (hid32[:, lanes] + mix32[...]).astype(BF16)
    stores.append(pltpu.make_async_copy(mixed, mixed_o, store.at[2]))
    stores[2].start()

    for copy in delta_copies + list(z_copies.values()) + list(b_copies.values()):
        copy.wait_send()
    for copies in gathers:
        for copy in copies.values():
            copy.wait_send()
    for copies in forwards + h_copies + r_copies:
        for copy in copies:
            copy.wait_send()
    for copy in stores:
        copy.wait()


def shards(*args):
    args = list(args)
    for i in (1, 14):
        args[i] = args[i].reshape(16, 128)
    args[10] = args[10].reshape(2, 128)
    for i in (6, 7):
        args[i] = args[i].transpose(0, 2, 1)
    args[15], args[16] = args[15].T, args[16].T
    held = []
    for i, arg in enumerate(args):
        if i in (5, 16):
            held.append(pltpu.SMEM(arg.shape, arg.dtype))
        elif i == 15:
            held.append(pltpu.SMEM((2, 128), arg.dtype))
        else:
            held.append(pltpu.VMEM(arg.shape, arg.dtype))
    dma = pltpu.SemaphoreType.DMA
    out_shapes = (
        jax.ShapeDtypeStruct((SEQ, QUARTER), BF16),
        jax.ShapeDtypeStruct((SEQ, GROUPS, STATE), F32),
        jax.ShapeDtypeStruct((SEQ, GROUPS, STATE), F32),
    )
    scratch = held + [
        pltpu.VMEM((SEQ, GROUPS, STATE), F32),
        pltpu.VMEM((SEQ, GROUPS, STATE), F32),
        pltpu.VMEM((SEQ, QUARTER), BF16),
        pltpu.VMEM((NY, SEQ, WIDTH), BF16),
        pltpu.VMEM((SEQ, WIDTH), F32),
        pltpu.VMEM((SEQ, WIDTH), F32),
        pltpu.VMEM((16, QUARTER), F32),
        pltpu.VMEM((8, 2, QUARTER), BF16),
        pltpu.VMEM((NZ, 2, QUARTER), BF16),
        pltpu.VMEM((2, NY, NC, NX, 16, QUARTER), BF16),
        pltpu.VMEM((2, 128, NY * HID), BF16),
        pltpu.VMEM((2, NC, NX, 16, QUARTER), BF16),
        pltpu.VMEM((2, NC, NX, 16, QUARTER), BF16),
        pltpu.VMEM((16, QUARTER), F32),
        pltpu.VMEM((2, 8, 2, QUARTER), BF16),
        pltpu.VMEM((NZ, 2, QUARTER), BF16),
        dma((20,)), dma((3,)),
        dma((NY,)), dma((NY,)), dma((NZ,)), dma((NZ,)),
        dma((2, NX, NY)), dma((2, NX, NY)), dma((2, NX, NY)), dma((2, NX, NY)),
        dma((2, NY)), dma((2, NY)), dma((2, NC, NX)), dma((2, NC, NX)), dma((NZ,)), dma((NZ,)),
        pltpu.VMEM((2 * NZ, QUARTER), F32),
        pltpu.VMEM((SEQ, QUARTER), F32),
    ]
    anywhere = pl.BlockSpec(memory_space=pl.ANY)
    return pl.pallas_call(
        kernel,
        out_shape=out_shapes,
        in_specs=[anywhere] * 20,
        out_specs=(anywhere,) * 3,
        scratch_shapes=scratch,
        compiler_params=pltpu.CompilerParams(collective_id=0, has_side_effects=True),
    )(*args)


def solution(mesh):
    in_specs = (
        P("ep", None), P(), P(None, "tp"), P("tp", None), P("tp", None), P("tp"),
        P("tp", None, None), P("tp", None, None), P("tp", None, None), P("tp", None, None), P("tp"),
        P("ep", "tp", None), P("ep", "tp", None), P("tp", None), P(), P(), P("ep", None),
        P(None, ("ep", "tp")), P(None, ("ep", "tp")), P("ep", "tp"),
    )
    out_specs = (P("ep", "tp"), P("ep", "tp", None), P("ep", "tp", None))
    return jax.shard_map(shards, mesh=mesh, in_specs=in_specs, out_specs=out_specs, check_vma=False)
```

time: 139 us -> 58.3 us (0.42); the launches traced: 137 us -> 58.1 us
  blocking collectives: 80.8 us -> 0 us
  Pallas kernels: 0 us -> 54.2 us
  waiting for transfers between devices: 21.4 us -> 0 us
  starting transfers between devices: 16.6 us -> 0 us
  local copies, waits for them, and re-layouts: 9.71 us -> 3.27 us
  matrix products: 6.13 us -> 0 us
  other arithmetic: 1.71 us -> 0 us
    all_to_all x2 -> x0, blocking collectives: 80.8 us -> none  [the longest x1 72.9 us: shards(): lax.all_to_all(jnp.repeat(outgoing, group_span, axis=0), 'ep', split_axis...]
    pallas_call x0 -> x1, Pallas kernels: none -> 54.2 us  [shards(): pl.pallas_call(kernel, out_shape=out_shapes, in_specs=[anywhere] * 20, ou...]
    all_to_all x2 -> x0, waiting for transfers between devices: 21.4 us -> none  [the longest x1 19.2 us: shards(): lax.all_to_all(rounded, 'ep', split_axis=0, concat_axis=0, tiled=True)]
    all_to_all x2 -> x0, starting transfers between devices: 16.6 us -> none  [the longest x1 11.6 us: shards(): lax.all_to_all(rounded, 'ep', split_axis=0, concat_axis=0, tiled=True)]
    dot_general x11 -> x0, matrix products: 6.13 us -> none  [the longest x1 1.55 us: shards(): jnp.dot(normed_in, in_weight, preferred_element_type=jnp.float32)]
    unnamed x34 -> x7, local copies, waits for them, and re-layouts: 5.13 us -> 3.27 us
  transfers between devices with their start and end apart: 2 -> 0, of which waited for: 2 -> 0; matrix products, arithmetic and copies ran while one was open for 2% -> 0% of each run, Pallas kernels for 0% -> 0%
where the time goes in v1:
time: 58.3 us; the launch traced here: 58.1 us
  Pallas kernels  54.2 us (93%)
  local copies, waits for them, and re-layouts  3.27 us (6%)
  between operations  0.66 us (1%)
    pallas_call x1, Pallas kernels, shards(): pl.pallas_call(kernel, out_shape=out_shapes, in_specs=[anywhere] * 20, ou...  54.2 us
    unnamed x7, local copies, waits for them, and re-layouts  3.27 us

profile of v1, /device:TPU:1, one launch (start us, length us, event | category | flops | bytes accessed | tf_op | source)
XLA Modules:
  0.0 58.1 jit_solution(798639810584591468)
XLA Ops:
  0.6 54.2 %shard_map.211 = (bf16[4,512]{1,0:T(4,128)(2,1)}, f32[4,16,64]{2,1,0:T(8,128)}, f32[4,16,64]{2,1,0:T(8,128)}) custom-call(bf16[4,2048]{1,0:T(4,128)(2,1)} %refs_0_.1, bf16[16,128]{1,0:T(8,128)(2,1)} %bitcast.9, bf16[2048,256]{1,0:T(8,128)(2,1)} %refs_2_.1, f32[16,64]{1,0:T(8,128)} %refs_3_.1, f32[16,64]{1,0:T(8,128)} %refs_4_.1, f32[16]{0:T(128)} %refs_5_.1, ...), custom_call_target="tpu_custom_call" | custom-call | tf_op jit(solution)/shard_map/pallas_call | solution.py:400
  54.8 0.0 copy-start.1
  54.8 0.7 %copy-done.1 = bf16[4,512]{1,0:T(4,128)(2,1)S(1)} copy-done((bf16[4,512]{1,0:T(4,128)(2,1)S(1)}, bf16[4,512]{1,0:T(4,128)(2,1)}, u32[]{:S(2)}) %copy-start.1) | copy-done | bytes 4120
  55.5 0.6 %copy.26 = bf16[4,512]{1,0:T(4,128)(2,1)} copy(bf16[4,512]{1,0:T(4,128)(2,1)S(1)} %copy-done.1) | data formatting | bytes 8192
  56.1 0.0 copy-start
  56.1 1.4 %copy.27 = f32[4,16,64]{2,1,0:T(8,128)} copy(f32[4,16,64]{2,1,0:T(8,128)} %get-tuple-element.7) | data formatting | bytes 32768
  57.5 0.0 copy-done
  57.5 0.6 %copy.28 = f32[4,16,64]{2,1,0:T(8,128)} copy(f32[4,16,64]{2,1,0:T(8,128)S(1)} %copy-done) | data formatting | bytes 32768
Async XLA Ops:
  54.8 0.7 %copy-start.1 = (bf16[4,512]{1,0:T(4,128)(2,1)S(1)}, bf16[4,512]{1,0:T(4,128)(2,1)}, u32[]{:S(2)}) copy-start(bf16[4,512]{1,0:T(4,128)(2,1)} %get-tuple-element.6) | copy-start | bytes 12292
  56.1 1.4 %copy-start = (f32[4,16,64]{2,1,0:T(8,128)S(1)}, f32[4,16,64]{2,1,0:T(8,128)}, u32[]{:S(2)}) copy-start(f32[4,16,64]{2,1,0:T(8,128)} %get-tuple-element.8) | copy-start | bytes 49156

commit v2 on v1

--- a/solution.py
+++ b/solution.py
@@ -12,7 +12,7 @@
 SEQ, WIDTH, QUARTER = 4, 2048, 512
 GROUPS, STATE, CHANNELS = 16, 64, 256
 HID = 128
-CHUNKS = ((0, 1, 15, 2, 14, 3, 13, 4), (12, 5, 11, 6, 10, 7, 9, 8))
+HALF = NZ // 2
 PLANE = sorted(
     [(dx, dy) for dx in range(NX) for dy in range(NY)],
     key=lambda d: min(d[0], NX - d[0]) + min(d[1], NY - d[1]),
@@ -57,6 +57,7 @@
     (gat, hid, send, recv, sum32, back, zout, load, store) = scratch[29:38]
     (ds_sem, dr_sem, zs_sem, zr_sem, gs_sem, gr_sem, fs_sem, fr_sem) = scratch[38:46]
     (hs_sem, hr_sem, rs_sem, rr_sem, bs_sem, br_sem) = scratch[46:52]
+    out32, mix32, near_sem, far_sem = scratch[52:56]
 
     ep, y = lax.axis_index("ep"), lax.axis_index("tp")
     z, x, c = ep // 8, (ep // 2) % NX, ep % 2
@@ -68,11 +69,20 @@
         return lax.rem(a + d, n)
 
     barrier = pltpu.get_barrier_semaphore()
-    partners = [at(turn(z, d, NZ), x, c, y) for d in range(1, NZ)]
-    partners += [at(z, turn(x, dx, NX), c, turn(y, dy, NY)) for dx, dy in PLANE if dx or dy]
-    partners += [at(z, turn(x, dx, NX), 1 - c, y) for dx in range(NX)]
-    for device in partners:
+
+    def enter(device):
         pl.semaphore_signal(barrier, inc=1, device_id=device, device_id_type=MESH)
+
+    for d in range(1, NY):
+        enter(at(z, x, 0, turn(y, d, NY)))
+    for d in range(1, NZ):
+        enter(at(turn(z, d, NZ), x, 1, y))
+    for dx, dy in PLANE:
+        if dx or dy:
+            enter(at(z, turn(x, dx, NX), 1, turn(y, dy, NY)))
+    enter(at(z, x, 1 - c, y))
+    near_count = 2 * (NY - 1) + 1
+    far_count = 2 * (NZ - 1) + 2 * (NX * NY - 1) + 1
 
     wide = pl.multiple_of((ep // 32) * 128, 128)
     sources = list(hbm)
@@ -145,7 +155,15 @@
     loads[13].wait()
     delta[y] = dot(activated, outw[...]).astype(BF16)
 
-    pl.semaphore_wait(barrier, len(partners))
+    @pl.when(c == 0)
+    def _():
+        pl.semaphore_wait(barrier, near_count)
+        pl.semaphore_signal(near_sem, inc=1, device_id=at(z, x, 1, y), device_id_type=MESH)
+
+    @pl.when(c == 1)
+    def _():
+        pl.semaphore_wait(near_sem, 1)
+
     delta_copies = [
         pltpu.make_async_remote_copy(
             delta.at[y], delta.at[y], ds_sem.at[d], dr_sem.at[d],
@@ -202,24 +220,39 @@
     for e in range(8):
         pick[e] = pick32[2 * e : 2 * e + 2, :].astype(BF16)
 
-    z_copies = {}
+    @pl.when(c == 1)
+    def _():
+        pl.semaphore_wait(barrier, far_count)
+        pl.semaphore_signal(far_sem, inc=1, device_id=at(z, x, 0, y), device_id_type=MESH)
+
+    @pl.when(c == 0)
+    def _():
+        pl.semaphore_wait(far_sem, 1)
+
+    z_copies = []
     for d in (8, 7, 9, 6, 10, 5, 11, 4, 12, 3, 13, 2, 14, 1, 15):
         to = turn(z, d, NZ)
-        z_copies[d] = pltpu.make_async_remote_copy(
-            pick.at[to // 2], zin.at[d], zs_sem.at[d], zr_sem.at[d],
-            device_id=at(to, x, c, y), device_id_type=MESH,
+        z_copies.append(
+            pltpu.make_async_remote_copy(
+                pick.at[to // 2], zin.at[z], zs_sem.at[d], zr_sem.at[z],
+                device_id=at(to, x, c, y), device_id_type=MESH,
+            )
         )
-        z_copies[d].start()
-
-    gathers, forwards = [], []
-    for k, chunk in enumerate(CHUNKS):
-        for i, d in enumerate(chunk):
-            if d:
-                z_copies[d].wait_recv()
-                piece = zin[d]
-            else:
-                piece = pick[z // 2]
-            sum32[2 * i : 2 * i + 2, :] = piece.astype(F32)
+        z_copies[-1].start()
+    pltpu.make_async_copy(pick.at[z // 2], zin.at[z], zr_sem.at[z]).start()
+
+    def landed(ref, sem):
+        pltpu.make_async_remote_copy(
+            ref, ref, zs_sem.at[0], sem, device_id=at(z, x, 1 - c, y), device_id_type=MESH
+        ).wait_recv()
+
+    gathers, forwards = [], {}
+
+    def gather_chunk(k):
+        for i in range(HALF):
+            home = k * HALF + i
+            landed(zin.at[home], zr_sem.at[home])
+            sum32[2 * i : 2 * i + 2, :] = zin[home].astype(F32)
         gat[k, y, c, x] = sum32[...].astype(BF16)
         copies = {}
         for dx, dy in reversed(PLANE):
@@ -231,7 +264,7 @@
                 copies[dx, dy].start()
         gathers.append(copies)
 
-    h_copies, r_copies = [], []
+    h_copies, r_copies = {}, {}
 
     def spread_chunk(k):
         copies = []
@@ -246,7 +279,7 @@
                 )
             )
             copies[-1].start()
-        forwards.append(copies)
+        forwards[k] = copies
 
     def up_chunk(k):
         for copy in forwards[k]:
@@ -268,7 +301,7 @@
                 )
             )
             copies[-1].start()
-        h_copies.append(copies)
+        h_copies[k] = copies
 
     def down_chunk(k):
         for copy in h_copies[k]:
@@ -286,7 +319,7 @@
                         )
                     )
                     copies[-1].start()
-        r_copies.append(copies)
+        r_copies[k] = copies
 
     b_copies = {}
 
@@ -299,16 +332,25 @@
                 if dx or dc:
                     total = total + recv[k, dc, dx].astype(F32)
         sum32[...] = total
-        for i, d in enumerate(CHUNKS[k]):
+        for i in range(HALF):
             back[k, i] = sum32[2 * i : 2 * i + 2, :].astype(BF16)
-        for i, d in reversed(list(enumerate(CHUNKS[k]))):
-            if d:
-                b_copies[d] = pltpu.make_async_remote_copy(
-                    back.at[k, i], zout.at[d], bs_sem.at[d], br_sem.at[d],
-                    device_id=at(turn(z, NZ - d, NZ), x, c, y), device_id_type=MESH,
-                )
-                b_copies[d].start()
-
+        for i in range(HALF):
+            home = k * HALF + i
+            b_copies[home] = pltpu.make_async_remote_copy(
+                back.at[k, i], zout.at[z], bs_sem.at[home], br_sem.at[z],
+                device_id=at(home, x, c, y), device_id_type=MESH,
+            )
+
+            @pl.when(z != home)
+            def _():
+                b_copies[home].start()
+
+            @pl.when(z == home)
+            def _():
+                pltpu.make_async_copy(back.at[k, i], zout.at[z], br_sem.at[z]).start()
+
+    gather_chunk(0)
+    gather_chunk(1)
     spread_chunk(0)
     loads[17].wait()
     loads[18].wait()
@@ -317,20 +359,15 @@
     loads[19].wait()
     down_chunk(0)
     up_chunk(1)
+    home_chunk(0)
     down_chunk(1)
-    home_chunk(0)
     home_chunk(1)
 
     back_row = iota((2 * NZ, QUARTER), 0)
-    _, scales = table(((z + back_row // 2) % NZ) // 2, back_row % 2, (2 * NZ, QUARTER))
-    out32, mix32 = scratch[52], scratch[53]
-    for d in (0, 1, 15, 2, 14, 3, 13, 4, 12, 5, 11, 6, 10, 7, 9, 8):
-        if d:
-            b_copies[d].wait_recv()
-            piece = zout[d]
-        else:
-            piece = back[0, 0]
-        out32[2 * d : 2 * d + 2, :] = piece.astype(F32)
+    _, scales = table(back_row // 4, back_row % 2, (2 * NZ, QUARTER))
+    for p in range(NZ):
+        landed(zout.at[p], br_sem.at[p])
+        out32[2 * p : 2 * p + 2, :] = zout[p].astype(F32)
     pieces = out32[...]
     for s in range(SEQ):
         mix32[s : s + 1, :] = jnp.sum(scales[s] * pieces, axis=0, keepdims=True)
@@ -338,13 +375,19 @@
     stores.append(pltpu.make_async_copy(mixed, mixed_o, store.at[2]))
     stores[2].start()
 
-    for copy in delta_copies + list(z_copies.values()) + list(b_copies.values()):
+    for copy in delta_copies + z_copies:
         copy.wait_send()
+    for home, copy in b_copies.items():
+
+        @pl.when(z != home)
+        def _():
+            copy.wait_send()
+
     for copies in gathers:
         for copy in copies.values():
             copy.wait_send()
-    for copies in forwards + h_copies + r_copies:
-        for copy in copies:
+    for copies in (forwards, h_copies, r_copies):
+        for copy in copies[0] + copies[1]:
             copy.wait_send()
     for copy in stores:
         copy.wait()
@@ -395,6 +438,8 @@
         dma((2, NY)), dma((2, NY)), dma((2, NC, NX)), dma((2, NC, NX)), dma((NZ,)), dma((NZ,)),
         pltpu.VMEM((2 * NZ, QUARTER), F32),
         pltpu.VMEM((SEQ, QUARTER), F32),
+        pltpu.SemaphoreType.REGULAR,
+        pltpu.SemaphoreType.REGULAR,
     ]
     anywhere = pl.BlockSpec(memory_space=pl.ANY)
     return pl.pallas_call(

time: 58.3 us -> 53.2 us (0.913)
  Pallas kernels: 54.2 us -> 49 us
    pallas_call x1, Pallas kernels: 54.2 us -> 49 us  [shards(): pl.pallas_call(kernel, out_shape=out_shapes, in_specs=[anywhere] * 20, ou...]
where the time goes in v2:
time: 53.2 us; the launch traced here: 53 us
  Pallas kernels  49 us (92%)
  local copies, waits for them, and re-layouts  3.27 us (6%)
  between operations  0.66 us (1%)
    pallas_call x1, Pallas kernels, shards(): pl.pallas_call(kernel, out_shape=out_shapes, in_specs=[anywhere] * 20, ou...  49 us
    unnamed x7, local copies, waits for them, and re-layouts  3.27 us

profile of v2, /device:TPU:1, one launch (start us, length us, event | category | flops | bytes accessed | tf_op | source)
XLA Modules:
  0.0 53.0 jit_solution(7359577909548237702)
XLA Ops:
  0.6 49.0 %shard_map.211 = (bf16[4,512]{1,0:T(4,128)(2,1)}, f32[4,16,64]{2,1,0:T(8,128)}, f32[4,16,64]{2,1,0:T(8,128)}) custom-call(bf16[4,2048]{1,0:T(4,128)(2,1)} %refs_0_.1, bf16[16,128]{1,0:T(8,128)(2,1)} %bitcast.9, bf16[2048,256]{1,0:T(8,128)(2,1)} %refs_2_.1, f32[16,64]{1,0:T(8,128)} %refs_3_.1, f32[16,64]{1,0:T(8,128)} %refs_4_.1, f32[16]{0:T(128)} %refs_5_.1, ...), custom_call_target="tpu_custom_call" | custom-call | tf_op jit(solution)/shard_map/pallas_call | solution.py:445
  49.7 0.0 copy-start.1
  49.7 0.7 %copy-done.1 = bf16[4,512]{1,0:T(4,128)(2,1)S(1)} copy-done((bf16[4,512]{1,0:T(4,128)(2,1)S(1)}, bf16[4,512]{1,0:T(4,128)(2,1)}, u32[]{:S(2)}) %copy-start.1) | copy-done | bytes 4120
  50.4 0.6 %copy.26 = bf16[4,512]{1,0:T(4,128)(2,1)} copy(bf16[4,512]{1,0:T(4,128)(2,1)S(1)} %copy-done.1) | data formatting | bytes 8192
  51.0 0.0 copy-start
  51.0 1.4 %copy.27 = f32[4,16,64]{2,1,0:T(8,128)} copy(f32[4,16,64]{2,1,0:T(8,128)} %get-tuple-element.7) | data formatting | bytes 32768
  52.3 0.0 copy-done
  52.3 0.6 %copy.28 = f32[4,16,64]{2,1,0:T(8,128)} copy(f32[4,16,64]{2,1,0:T(8,128)S(1)} %copy-done) | data formatting | bytes 32768
Async XLA Ops:
  49.7 0.7 %copy-start.1 = (bf16[4,512]{1,0:T(4,128)(2,1)S(1)}, bf16[4,512]{1,0:T(4,128)(2,1)}, u32[]{:S(2)}) copy-start(bf16[4,512]{1,0:T(4,128)(2,1)} %get-tuple-element.6) | copy-start | bytes 12292
  51.0 1.4 %copy-start = (f32[4,16,64]{2,1,0:T(8,128)S(1)}, f32[4,16,64]{2,1,0:T(8,128)}, u32[]{:S(2)}) copy-start(f32[4,16,64]{2,1,0:T(8,128)} %get-tuple-element.8) | copy-start | bytes 49156

commit v3 on v2

--- a/solution.py
+++ b/solution.py
@@ -13,6 +13,8 @@
 GROUPS, STATE, CHANNELS = 16, 64, 256
 HID = 128
 HALF = NZ // 2
+VMEM_LIMIT = 67043328 - 72 * 1024
+LOAD_GROUP = (0, 0, 1, 2, 2, 2, 2, 2, 4, 4, 4, 3, 3, 5, 6, 6, 6, 7, 7, 8)
 PLANE = sorted(
     [(dx, dy) for dx in range(NX) for dy in range(NY)],
     key=lambda d: min(d[0], NX - d[0]) + min(d[1], NY - d[1]),
@@ -53,11 +55,10 @@
     mixed_o, newr_o, newi_o = outs
     (tok, gain, inw, decay, freq, steps, inr, ini, outr, outi) = scratch[:10]
     (skip, st_r, st_i, outw, fgain, ids, rw, gw, uw, dw) = scratch[10:20]
-    (newr, newi, mixed, delta, norm32, hid32, pick32, pick, zin) = scratch[20:29]
-    (gat, hid, send, recv, sum32, back, zout, load, store) = scratch[29:38]
-    (ds_sem, dr_sem, zs_sem, zr_sem, gs_sem, gr_sem, fs_sem, fr_sem) = scratch[38:46]
-    (hs_sem, hr_sem, rs_sem, rr_sem, bs_sem, br_sem) = scratch[46:52]
-    out32, mix32, near_sem, far_sem = scratch[52:56]
+    (delta, norm32, hid32, pick32, pick, zin) = scratch[20:26]
+    (gat, hid, send, recv, sum32, back, zout, out32) = scratch[26:34]
+    load, sent, dr_sem, zr_sem, gr_sem, fr_sem, hr_sem, rr_sem, br_sem, near_sem, far_sem = scratch[34:]
+    D_SENT, Z_SENT, G_SENT, F_SENT, H_SENT, R_SENT, B_SENT = (sent.at[i] for i in range(7))
 
     ep, y = lax.axis_index("ep"), lax.axis_index("tp")
     z, x, c = ep // 8, (ep // 2) % NX, ep % 2
@@ -67,6 +68,11 @@
 
     def turn(a, d, n):
         return lax.rem(a + d, n)
+
+    def landed(ref, sem):
+        pltpu.make_async_remote_copy(
+            ref, ref, D_SENT, sem, device_id=at(z, x, 1 - c, y), device_id_type=MESH
+        ).wait_recv()
 
     barrier = pltpu.get_barrier_semaphore()
 
@@ -88,7 +94,7 @@
     sources = list(hbm)
     sources[15] = ids_h.at[:, pl.ds(wide, 128)]
     loads = [
-        pltpu.make_async_copy(source, target, load.at[i])
+        pltpu.make_async_copy(source, target, load.at[LOAD_GROUP[i]])
         for i, (source, target) in enumerate(zip(sources, scratch[:20]))
     ]
     for i in (0, 1, 2, 3, 4, 5, 6, 7, 11, 12, 8, 9, 10, 13, 14, 15, 16, 17, 18, 19):
@@ -137,8 +143,8 @@
     state_r, state_i = st_r[...].reshape(rows, STATE), st_i[...].reshape(rows, STATE)
     new_r = (bar_real * state_r - bar_imag * state_i) + (factor_real * drive_r - factor_imag * drive_i)
     new_i = (bar_real * state_i + bar_imag * state_r) + (factor_real * drive_i + factor_imag * drive_r)
-    newr[...] = new_r.reshape(SEQ, GROUPS, STATE)
-    newi[...] = new_i.reshape(SEQ, GROUPS, STATE)
+    newr_o[...] = new_r.reshape(SEQ, GROUPS, STATE)
+    newi_o[...] = new_i.reshape(SEQ, GROUPS, STATE)
 
     for i in (8, 9, 10):
         loads[i].wait()
@@ -166,18 +172,12 @@
 
     delta_copies = [
         pltpu.make_async_remote_copy(
-            delta.at[y], delta.at[y], ds_sem.at[d], dr_sem.at[d],
+            delta.at[y], delta.at[y], D_SENT, dr_sem,
             device_id=at(z, x, c, turn(y, d, NY)), device_id_type=MESH,
         )
         for d in range(1, NY)
     ]
     for copy in delta_copies:
-        copy.start()
-    stores = [
-        pltpu.make_async_copy(newr, newr_o, store.at[0]),
-        pltpu.make_async_copy(newi, newi_o, store.at[1]),
-    ]
-    for copy in stores:
         copy.start()
 
     for i in (14, 15, 16):
@@ -203,8 +203,7 @@
     picks, _ = table(pick_row // 2, pick_row % 2, (16, QUARTER))
     ffn_gain = row_of(fgain[...])
 
-    for copy in delta_copies:
-        copy.wait_recv()
+    landed(delta.at[0 : NY - 1], dr_sem)
     total = tokens
     for i in range(NY):
         total = total + delta[i].astype(F32)
@@ -234,56 +233,50 @@
         to = turn(z, d, NZ)
         z_copies.append(
             pltpu.make_async_remote_copy(
-                pick.at[to // 2], zin.at[z], zs_sem.at[d], zr_sem.at[z],
+                pick.at[to // 2], zin.at[z], Z_SENT, zr_sem.at[z // HALF],
                 device_id=at(to, x, c, y), device_id_type=MESH,
             )
         )
         z_copies[-1].start()
-    pltpu.make_async_copy(pick.at[z // 2], zin.at[z], zr_sem.at[z]).start()
-
-    def landed(ref, sem):
-        pltpu.make_async_remote_copy(
-            ref, ref, zs_sem.at[0], sem, device_id=at(z, x, 1 - c, y), device_id_type=MESH
-        ).wait_recv()
+    pltpu.make_async_copy(pick.at[z // 2], zin.at[z], zr_sem.at[z // HALF]).start()
 
     gathers, forwards = [], {}
 
     def gather_chunk(k):
+        landed(zin.at[k * HALF : (k + 1) * HALF], zr_sem.at[k])
         for i in range(HALF):
-            home = k * HALF + i
-            landed(zin.at[home], zr_sem.at[home])
-            sum32[2 * i : 2 * i + 2, :] = zin[home].astype(F32)
+            sum32[2 * i : 2 * i + 2, :] = zin[k * HALF + i].astype(F32)
         gat[k, y, c, x] = sum32[...].astype(BF16)
-        copies = {}
+        copies = []
         for dx, dy in reversed(PLANE):
             if dx or dy:
-                copies[dx, dy] = pltpu.make_async_remote_copy(
-                    gat.at[k, y, c, x], gat.at[k, y, c, x], gs_sem.at[k, dx, dy], gr_sem.at[k, dx, dy],
-                    device_id=at(z, turn(x, dx, NX), c, turn(y, dy, NY)), device_id_type=MESH,
+                copies.append(
+                    pltpu.make_async_remote_copy(
+                        gat.at[k, y, c, x], gat.at[k, y, c, x], G_SENT, gr_sem.at[k, dx],
+                        device_id=at(z, turn(x, dx, NX), c, turn(y, dy, NY)), device_id_type=MESH,
+                    )
                 )
-                copies[dx, dy].start()
+                copies[-1].start()
         gathers.append(copies)
 
     h_copies, r_copies = {}, {}
 
     def spread_chunk(k):
         copies = []
-        for dx, dy in PLANE:
-            if dx or dy:
-                gathers[k][dx, dy].wait_recv()
-            slot = gat.at[k, turn(y, NY - dy, NY), c, turn(x, NX - dx, NX)]
+        for dx in (0, 1, 3, 2):
+            rows_x = turn(x, NX - dx, NX)
+            landed(gat.at[k, (0 if dx else 1) : NY, c, rows_x], gr_sem.at[k, dx])
+            slots = gat.at[k, :, c, rows_x]
             copies.append(
                 pltpu.make_async_remote_copy(
-                    slot, slot, fs_sem.at[k, dx, dy], fr_sem.at[k, dx, dy],
-                    device_id=at(z, x, 1 - c, y), device_id_type=MESH,
+                    slots, slots, F_SENT, fr_sem.at[k], device_id=at(z, x, 1 - c, y), device_id_type=MESH
                 )
             )
             copies[-1].start()
         forwards[k] = copies
 
     def up_chunk(k):
-        for copy in forwards[k]:
-            copy.wait_recv()
+        landed(gat.at[k, :, 1 - c], fr_sem.at[k])
         gate_pre = jnp.zeros((128, HID), F32)
         up_pre = jnp.zeros((128, HID), F32)
         for q in range(NY):
@@ -296,7 +289,7 @@
         for d in (2, 1, 3):
             copies.append(
                 pltpu.make_async_remote_copy(
-                    hid.at[k, :, units], hid.at[k, :, units], hs_sem.at[k, d], hr_sem.at[k, d],
+                    hid.at[k, :, units], hid.at[k, :, units], H_SENT, hr_sem.at[k],
                     device_id=at(z, x, c, turn(y, d, NY)), device_id_type=MESH,
                 )
             )
@@ -304,8 +297,7 @@
         h_copies[k] = copies
 
     def down_chunk(k):
-        for copy in h_copies[k]:
-            copy.wait_recv()
+        landed(hid.at[k, :, 0 : (NY - 1) * HID], hr_sem.at[k])
         send[k] = dot(hid[k], dw[...]).astype(BF16).reshape(NC, NX, 16, QUARTER)
         copies = []
         for dx in (2, 1, 3, 0):
@@ -314,7 +306,7 @@
                     to_x, to_c = turn(x, dx, NX), c if dc == 0 else 1 - c
                     copies.append(
                         pltpu.make_async_remote_copy(
-                            send.at[k, to_c, to_x], recv.at[k, dc, dx], rs_sem.at[k, dc, dx], rr_sem.at[k, dc, dx],
+                            send.at[k, to_c, to_x], recv.at[k, dc * NX + dx - 1], R_SENT, rr_sem.at[k],
                             device_id=at(z, to_x, to_c, y), device_id_type=MESH,
                         )
                     )
@@ -324,20 +316,17 @@
     b_copies = {}
 
     def home_chunk(k):
-        for copy in r_copies[k]:
-            copy.wait_recv()
+        landed(recv.at[k], rr_sem.at[k])
         total = send[k, c, x].astype(F32)
-        for dc in range(NC):
-            for dx in range(NX):
-                if dx or dc:
-                    total = total + recv[k, dc, dx].astype(F32)
+        for i in range(NC * NX - 1):
+            total = total + recv[k, i].astype(F32)
         sum32[...] = total
         for i in range(HALF):
             back[k, i] = sum32[2 * i : 2 * i + 2, :].astype(BF16)
         for i in range(HALF):
             home = k * HALF + i
             b_copies[home] = pltpu.make_async_remote_copy(
-                back.at[k, i], zout.at[z], bs_sem.at[home], br_sem.at[z],
+                back.at[k, i], zout.at[z], B_SENT, br_sem,
                 device_id=at(home, x, c, y), device_id_type=MESH,
             )
 
@@ -347,7 +336,7 @@
 
             @pl.when(z == home)
             def _():
-                pltpu.make_async_copy(back.at[k, i], zout.at[z], br_sem.at[z]).start()
+                pltpu.make_async_copy(back.at[k, i], zout.at[z], br_sem).start()
 
     gather_chunk(0)
     gather_chunk(1)
@@ -356,24 +345,21 @@
     loads[18].wait()
     up_chunk(0)
     spread_chunk(1)
+    up_chunk(1)
     loads[19].wait()
     down_chunk(0)
-    up_chunk(1)
+    down_chunk(1)
     home_chunk(0)
-    down_chunk(1)
     home_chunk(1)
 
     back_row = iota((2 * NZ, QUARTER), 0)
     _, scales = table(back_row // 4, back_row % 2, (2 * NZ, QUARTER))
+    landed(zout, br_sem)
     for p in range(NZ):
-        landed(zout.at[p], br_sem.at[p])
         out32[2 * p : 2 * p + 2, :] = zout[p].astype(F32)
     pieces = out32[...]
-    for s in range(SEQ):
-        mix32[s : s + 1, :] = jnp.sum(scales[s] * pieces, axis=0, keepdims=True)
-    mixed[...] = (hid32[:, lanes] + mix32[...]).astype(BF16)
-    stores.append(pltpu.make_async_copy(mixed, mixed_o, store.at[2]))
-    stores[2].start()
+    routed = [jnp.sum(scales[s] * pieces, axis=0, keepdims=True) for s in range(SEQ)]
+    mixed_o[...] = (hid32[:, lanes] + jnp.concatenate(routed, axis=0)).astype(BF16)
 
     for copy in delta_copies + z_copies:
         copy.wait_send()
@@ -383,13 +369,17 @@
         def _():
             copy.wait_send()
 
-    for copies in gathers:
-        for copy in copies.values():
+    for copies in gathers + [group[k] for group in (forwards, h_copies, r_copies) for k in range(2)]:
+        for copy in copies:
             copy.wait_send()
-    for copies in (forwards, h_copies, r_copies):
-        for copy in copies[0] + copies[1]:
-            copy.wait_send()
-    for copy in stores:
+
+
+def store_kernel(*refs):
+    sources, targets, sem = refs[:3], refs[3:6], refs[6]
+    copies = [pltpu.make_async_copy(s, t, sem.at[i]) for i, (s, t) in enumerate(zip(sources, targets))]
+    for copy in copies:
+        copy.start()
+    for copy in copies:
         copy.wait()
 
 
@@ -410,15 +400,8 @@
         else:
             held.append(pltpu.VMEM(arg.shape, arg.dtype))
     dma = pltpu.SemaphoreType.DMA
-    out_shapes = (
-        jax.ShapeDtypeStruct((SEQ, QUARTER), BF16),
-        jax.ShapeDtypeStruct((SEQ, GROUPS, STATE), F32),
-        jax.ShapeDtypeStruct((SEQ, GROUPS, STATE), F32),
-    )
+    shapes = (((SEQ, QUARTER), BF16), ((SEQ, GROUPS, STATE), F32), ((SEQ, GROUPS, STATE), F32))
     scratch = held + [
-        pltpu.VMEM((SEQ, GROUPS, STATE), F32),
-        pltpu.VMEM((SEQ, GROUPS, STATE), F32),
-        pltpu.VMEM((SEQ, QUARTER), BF16),
         pltpu.VMEM((NY, SEQ, WIDTH), BF16),
         pltpu.VMEM((SEQ, WIDTH), F32),
         pltpu.VMEM((SEQ, WIDTH), F32),
@@ -428,28 +411,36 @@
         pltpu.VMEM((2, NY, NC, NX, 16, QUARTER), BF16),
         pltpu.VMEM((2, 128, NY * HID), BF16),
         pltpu.VMEM((2, NC, NX, 16, QUARTER), BF16),
-        pltpu.VMEM((2, NC, NX, 16, QUARTER), BF16),
+        pltpu.VMEM((2, NC * NX - 1, 16, QUARTER), BF16),
         pltpu.VMEM((16, QUARTER), F32),
         pltpu.VMEM((2, 8, 2, QUARTER), BF16),
         pltpu.VMEM((NZ, 2, QUARTER), BF16),
-        dma((20,)), dma((3,)),
-        dma((NY,)), dma((NY,)), dma((NZ,)), dma((NZ,)),
-        dma((2, NX, NY)), dma((2, NX, NY)), dma((2, NX, NY)), dma((2, NX, NY)),
-        dma((2, NY)), dma((2, NY)), dma((2, NC, NX)), dma((2, NC, NX)), dma((NZ,)), dma((NZ,)),
         pltpu.VMEM((2 * NZ, QUARTER), F32),
-        pltpu.VMEM((SEQ, QUARTER), F32),
+        dma((9,)), dma((7,)),
+        dma, dma((2,)), dma((2, NX)), dma((2,)), dma((2,)), dma((2,)), dma,
         pltpu.SemaphoreType.REGULAR,
         pltpu.SemaphoreType.REGULAR,
     ]
     anywhere = pl.BlockSpec(memory_space=pl.ANY)
+    near = pl.BlockSpec(memory_space=pltpu.VMEM)
+    results = pl.pallas_call(
+        kernel,
+        out_shape=tuple(pltpu.VMEM(*shape) for shape in shapes),
+        in_specs=[anywhere] * 20,
+        out_specs=(near,) * 3,
+        scratch_shapes=scratch,
+        compiler_params=pltpu.CompilerParams(
+            collective_id=0, has_side_effects=True, vmem_limit_bytes=VMEM_LIMIT
+        ),
+    )(*args)
     return pl.pallas_call(
-        kernel,
-        out_shape=out_shapes,
-        in_specs=[anywhere] * 20,
+        store_kernel,
+        out_shape=tuple(jax.ShapeDtypeStruct(*shape) for shape in shapes),
+        in_specs=[anywhere] * 3,
         out_specs=(anywhere,) * 3,
-        scratch_shapes=scratch,
-        compiler_params=pltpu.CompilerParams(collective_id=0, has_side_effects=True),
-    )(*args)
+        scratch_shapes=[dma((3,))],
+        compiler_params=pltpu.CompilerParams(vmem_limit_bytes=VMEM_LIMIT),
+    )(*[pltpu.with_memory_space_constraint(r, pltpu.VMEM) for r in results])
 
 
 def solution(mesh):

time: 53.2 us -> 47.9 us (0.900)
  local copies, waits for them, and re-layouts: 3.27 us -> 0 us
  Pallas kernels: 49 us -> 47.1 us
    unnamed x7 -> x0, local copies, waits for them, and re-layouts: 3.27 us -> none
    pallas_call x1 -> x2, Pallas kernels: 49 us -> 47.1 us  [the longest x1 46.5 us: shards(): pl.pallas_call(kernel, out_shape=tuple((pltpu.VMEM(*shape) for shape in s...]
where the time goes in v3:
time: 47.9 us; the launch traced here: 47.8 us
  Pallas kernels  47.1 us (98%)
  between operations  0.65 us (1%)
    pallas_call x1, Pallas kernels, shards(): pl.pallas_call(kernel, out_shape=tuple((pltpu.VMEM(*shape) for shape in s...  46.5 us

profile of v3, /device:TPU:1, one launch (start us, length us, event | category | flops | bytes accessed | tf_op | source)
XLA Modules:
  0.0 47.8 jit_solution(4874639952925521402)
XLA Ops:
  0.6 46.5 %shard_map.211 = (bf16[4,512]{1,0:T(4,128)(2,1)S(1)}, f32[4,16,64]{2,1,0:T(8,128)S(1)}, f32[4,16,64]{2,1,0:T(8,128)S(1)}) custom-call(bf16[4,2048]{1,0:T(4,128)(2,1)} %refs_0_.1, bf16[16,128]{1,0:T(8,128)(2,1)} %bitcast.9, bf16[2048,256]{1,0:T(8,128)(2,1)} %refs_2_.1, f32[16,64]{1,0:T(8,128)} %refs_3_.1, f32[16,64]{1,0:T(8,128)} %refs_4_.1, f32[16]{0:T(128)} %refs_5_.1, ...), custom_call_target="tpu_custom_call" | custom-call | tf_op jit(solution)/shard_map/pallas_call | solution.py:426
  47.1 0.7 %shard_map.212 = (bf16[4,512]{1,0:T(4,128)(2,1)}, f32[4,16,64]{2,1,0:T(8,128)}, f32[4,16,64]{2,1,0:T(8,128)}) custom-call(bf16[4,512]{1,0:T(4,128)(2,1)S(1)} %get-tuple-element.6.refs_0_, f32[4,16,64]{2,1,0:T(8,128)S(1)} %get-tuple-element.7.refs_1_, f32[4,16,64]{2,1,0:T(8,128)S(1)} %get-tuple-element.8.refs_2_), custom_call_target="tpu_custom_call" | custom-call | tf_op jit(solution)/shard_map/pallas_call | solution.py:436

commit v4 on v3

--- a/solution.py
+++ b/solution.py
@@ -13,6 +13,7 @@
 GROUPS, STATE, CHANNELS = 16, 64, 256
 HID = 128
 HALF = NZ // 2
+FAR_FIRST = (8, 7, 9, 6, 10, 5, 11, 4, 12, 3, 13, 2, 14, 1, 15)
 VMEM_LIMIT = 67043328 - 72 * 1024
 LOAD_GROUP = (0, 0, 1, 2, 2, 2, 2, 2, 4, 4, 4, 3, 3, 5, 6, 6, 6, 7, 7, 8)
 PLANE = sorted(
@@ -79,10 +80,10 @@
     def enter(device):
         pl.semaphore_signal(barrier, inc=1, device_id=device, device_id_type=MESH)
 
+    for d in FAR_FIRST:
+        enter(at(turn(z, d, NZ), x, 1, y))
     for d in range(1, NY):
         enter(at(z, x, 0, turn(y, d, NY)))
-    for d in range(1, NZ):
-        enter(at(turn(z, d, NZ), x, 1, y))
     for dx, dy in PLANE:
         if dx or dy:
             enter(at(z, turn(x, dx, NX), 1, turn(y, dy, NY)))
@@ -229,7 +230,7 @@
         pl.semaphore_wait(far_sem, 1)
 
     z_copies = []
-    for d in (8, 7, 9, 6, 10, 5, 11, 4, 12, 3, 13, 2, 14, 1, 15):
+    for d in FAR_FIRST:
         to = turn(z, d, NZ)
         z_copies.append(
             pltpu.make_async_remote_copy(
@@ -240,40 +241,48 @@
         z_copies[-1].start()
     pltpu.make_async_copy(pick.at[z // 2], zin.at[z], zr_sem.at[z // HALF]).start()
 
-    gathers, forwards = [], {}
-
-    def gather_chunk(k):
+    gathers, forwards = [], []
+
+    def take_chunk(k):
         landed(zin.at[k * HALF : (k + 1) * HALF], zr_sem.at[k])
         for i in range(HALF):
             sum32[2 * i : 2 * i + 2, :] = zin[k * HALF + i].astype(F32)
         gat[k, y, c, x] = sum32[...].astype(BF16)
-        copies = []
+
+    def pass_on(slots, k, dx, dy):
+        copy = pltpu.make_async_remote_copy(
+            slots, slots, G_SENT, gr_sem.at[k, dx],
+            device_id=at(z, turn(x, dx, NX), c, turn(y, dy, NY)), device_id_type=MESH,
+        )
+        copy.start()
+        gathers.append(copy)
+
+    def gather_at_once(k):
         for dx, dy in reversed(PLANE):
             if dx or dy:
-                copies.append(
-                    pltpu.make_async_remote_copy(
-                        gat.at[k, y, c, x], gat.at[k, y, c, x], G_SENT, gr_sem.at[k, dx],
-                        device_id=at(z, turn(x, dx, NX), c, turn(y, dy, NY)), device_id_type=MESH,
-                    )
-                )
-                copies[-1].start()
-        gathers.append(copies)
+                pass_on(gat.at[k, y, c, x], k, dx, dy)
+
+    def gather_along_y(k):
+        for dy in (2, 1, 3):
+            pass_on(gat.at[k, y, c, x], k, 0, dy)
+
+    def gather_along_x(k):
+        spread_chunk(k, (0,))
+        for dx in (2, 1, 3):
+            pass_on(gat.at[k, :, c, x], k, dx, 0)
 
     h_copies, r_copies = {}, {}
 
-    def spread_chunk(k):
-        copies = []
-        for dx in (0, 1, 3, 2):
+    def spread_chunk(k, distances):
+        for dx in distances:
             rows_x = turn(x, NX - dx, NX)
             landed(gat.at[k, (0 if dx else 1) : NY, c, rows_x], gr_sem.at[k, dx])
             slots = gat.at[k, :, c, rows_x]
-            copies.append(
-                pltpu.make_async_remote_copy(
-                    slots, slots, F_SENT, fr_sem.at[k], device_id=at(z, x, 1 - c, y), device_id_type=MESH
-                )
+            copy = pltpu.make_async_remote_copy(
+                slots, slots, F_SENT, fr_sem.at[k], device_id=at(z, x, 1 - c, y), device_id_type=MESH
             )
-            copies[-1].start()
-        forwards[k] = copies
+            copy.start()
+            forwards.append(copy)
 
     def up_chunk(k):
         landed(gat.at[k, :, 1 - c], fr_sem.at[k])
@@ -338,18 +347,21 @@
             def _():
                 pltpu.make_async_copy(back.at[k, i], zout.at[z], br_sem).start()
 
-    gather_chunk(0)
-    gather_chunk(1)
-    spread_chunk(0)
+    take_chunk(0)
+    gather_at_once(0)
+    take_chunk(1)
+    gather_along_y(1)
+    spread_chunk(0, (0, 1, 3, 2))
+    gather_along_x(1)
     loads[17].wait()
     loads[18].wait()
     up_chunk(0)
-    spread_chunk(1)
-    up_chunk(1)
     loads[19].wait()
     down_chunk(0)
+    spread_chunk(1, (1, 3, 2))
+    up_chunk(1)
+    home_chunk(0)
     down_chunk(1)
-    home_chunk(0)
     home_chunk(1)
 
     back_row = iota((2 * NZ, QUARTER), 0)
@@ -369,9 +381,8 @@
         def _():
             copy.wait_send()
 
-    for copies in gathers + [group[k] for group in (forwards, h_copies, r_copies) for k in range(2)]:
-        for copy in copies:
-            copy.wait_send()
+    for copy in gathers + forwards + h_copies[0] + h_copies[1] + r_copies[0] + r_copies[1]:
+        copy.wait_send()
 
 
 def store_kernel(*refs):

time: 47.9 us -> 47.3 us (0.987)
  Pallas kernels: 47.1 us -> 46.4 us
    pallas_call x1, Pallas kernels: 46.5 us -> 45.8 us  [shards(): pl.pallas_call(kernel, out_shape=tuple((pltpu.VMEM(*shape) for shape in s...]
where the time goes in v4:
time: 47.3 us; the launch traced here: 47.1 us
  Pallas kernels  46.4 us (98%)
  between operations  0.65 us (1%)
    pallas_call x1, Pallas kernels, shards(): pl.pallas_call(kernel, out_shape=tuple((pltpu.VMEM(*shape) for shape in s...  45.8 us

profile of v4, /device:TPU:1, one launch (start us, length us, event | category | flops | bytes accessed | tf_op | source)
XLA Modules:
  0.0 47.1 jit_solution(5033650303833927071)
XLA Ops:
  0.6 45.8 %shard_map.211 = (bf16[4,512]{1,0:T(4,128)(2,1)S(1)}, f32[4,16,64]{2,1,0:T(8,128)S(1)}, f32[4,16,64]{2,1,0:T(8,128)S(1)}) custom-call(bf16[4,2048]{1,0:T(4,128)(2,1)} %refs_0_.1, bf16[16,128]{1,0:T(8,128)(2,1)} %bitcast.9, bf16[2048,256]{1,0:T(8,128)(2,1)} %refs_2_.1, f32[16,64]{1,0:T(8,128)} %refs_3_.1, f32[16,64]{1,0:T(8,128)} %refs_4_.1, f32[16]{0:T(128)} %refs_5_.1, ...), custom_call_target="tpu_custom_call" | custom-call | tf_op jit(solution)/shard_map/pallas_call | solution.py:437
  46.4 0.7 %shard_map.212 = (bf16[4,512]{1,0:T(4,128)(2,1)}, f32[4,16,64]{2,1,0:T(8,128)}, f32[4,16,64]{2,1,0:T(8,128)}) custom-call(bf16[4,512]{1,0:T(4,128)(2,1)S(1)} %get-tuple-element.6.refs_0_, f32[4,16,64]{2,1,0:T(8,128)S(1)} %get-tuple-element.7.refs_1_, f32[4,16,64]{2,1,0:T(8,128)S(1)} %get-tuple-element.8.refs_2_), custom_call_target="tpu_custom_call" | custom-call | tf_op jit(solution)/shard_map/pallas_call | solution.py:447

commit v5 on v4

--- a/solution.py
+++ b/solution.py
@@ -12,7 +12,7 @@
 SEQ, WIDTH, QUARTER = 4, 2048, 512
 GROUPS, STATE, CHANNELS = 16, 64, 256
 HID = 128
-HALF = NZ // 2
+CHUNKS = ((0, 4), (4, 8), (8, 16))
 FAR_FIRST = (8, 7, 9, 6, 10, 5, 11, 4, 12, 3, 13, 2, 14, 1, 15)
 VMEM_LIMIT = 67043328 - 72 * 1024
 LOAD_GROUP = (0, 0, 1, 2, 2, 2, 2, 2, 4, 4, 4, 3, 3, 5, 6, 6, 6, 7, 7, 8)
@@ -57,8 +57,9 @@
     (tok, gain, inw, decay, freq, steps, inr, ini, outr, outi) = scratch[:10]
     (skip, st_r, st_i, outw, fgain, ids, rw, gw, uw, dw) = scratch[10:20]
     (delta, norm32, hid32, pick32, pick, zin) = scratch[20:26]
-    (gat, hid, send, recv, sum32, back, zout, out32) = scratch[26:34]
-    load, sent, dr_sem, zr_sem, gr_sem, fr_sem, hr_sem, rr_sem, br_sem, near_sem, far_sem = scratch[34:]
+    sum32, zout, out32 = scratch[26:29]
+    load, sent, dr_sem, zr_sem, gr_sem, fr_sem, hr_sem, rr_sem, br_sem, near_sem, far_sem = scratch[29:40]
+    gat, hid, send, recv, back = (scratch[40 + i :: 5] for i in range(5))
     D_SENT, Z_SENT, G_SENT, F_SENT, H_SENT, R_SENT, B_SENT = (sent.at[i] for i in range(7))
 
     ep, y = lax.axis_index("ep"), lax.axis_index("tp")
@@ -66,6 +67,9 @@
 
     def at(zz, xx, cc, yy):
         return (zz * 8 + xx * 2 + cc, yy)
+
+    def chunk_of(home):
+        return lax.min(home // 4, 2)
 
     def turn(a, d, n):
         return lax.rem(a + d, n)
@@ -234,20 +238,21 @@
         to = turn(z, d, NZ)
         z_copies.append(
             pltpu.make_async_remote_copy(
-                pick.at[to // 2], zin.at[z], Z_SENT, zr_sem.at[z // HALF],
+                pick.at[to // 2], zin.at[z], Z_SENT, zr_sem.at[chunk_of(z)],
                 device_id=at(to, x, c, y), device_id_type=MESH,
             )
         )
         z_copies[-1].start()
-    pltpu.make_async_copy(pick.at[z // 2], zin.at[z], zr_sem.at[z // HALF]).start()
+    pltpu.make_async_copy(pick.at[z // 2], zin.at[z], zr_sem.at[chunk_of(z)]).start()
 
     gathers, forwards = [], []
 
     def take_chunk(k):
-        landed(zin.at[k * HALF : (k + 1) * HALF], zr_sem.at[k])
-        for i in range(HALF):
-            sum32[2 * i : 2 * i + 2, :] = zin[k * HALF + i].astype(F32)
-        gat[k, y, c, x] = sum32[...].astype(BF16)
+        low, high = CHUNKS[k]
+        landed(zin.at[low:high], zr_sem.at[k])
+        for i in range(high - low):
+            sum32[2 * i : 2 * i + 2, :] = zin[low + i].astype(F32)
+        gat[k][y, c, x] = sum32[0 : 2 * (high - low), :].astype(BF16)
 
     def pass_on(slots, k, dx, dy):
         copy = pltpu.make_async_remote_copy(
@@ -260,24 +265,24 @@
     def gather_at_once(k):
         for dx, dy in reversed(PLANE):
             if dx or dy:
-                pass_on(gat.at[k, y, c, x], k, dx, dy)
+                pass_on(gat[k].at[y, c, x], k, dx, dy)
 
     def gather_along_y(k):
         for dy in (2, 1, 3):
-            pass_on(gat.at[k, y, c, x], k, 0, dy)
+            pass_on(gat[k].at[y, c, x], k, 0, dy)
 
     def gather_along_x(k):
         spread_chunk(k, (0,))
         for dx in (2, 1, 3):
-            pass_on(gat.at[k, :, c, x], k, dx, 0)
+            pass_on(gat[k].at[:, c, x], k, dx, 0)
 
     h_copies, r_copies = {}, {}
 
     def spread_chunk(k, distances):
         for dx in distances:
             rows_x = turn(x, NX - dx, NX)
-            landed(gat.at[k, (0 if dx else 1) : NY, c, rows_x], gr_sem.at[k, dx])
-            slots = gat.at[k, :, c, rows_x]
+            landed(gat[k].at[(0 if dx else 1) : NY, c, rows_x], gr_sem.at[k, dx])
+            slots = gat[k].at[:, c, rows_x]
             copy = pltpu.make_async_remote_copy(
                 slots, slots, F_SENT, fr_sem.at[k], device_id=at(z, x, 1 - c, y), device_id_type=MESH
             )
@@ -285,20 +290,21 @@
             forwards.append(copy)
 
     def up_chunk(k):
-        landed(gat.at[k, :, 1 - c], fr_sem.at[k])
-        gate_pre = jnp.zeros((128, HID), F32)
-        up_pre = jnp.zeros((128, HID), F32)
+        landed(gat[k].at[:, 1 - c], fr_sem.at[k])
+        rows = hid[k].shape[0]
+        gate_pre = jnp.zeros((rows, HID), F32)
+        up_pre = jnp.zeros((rows, HID), F32)
         for q in range(NY):
-            block = gat[k, q].reshape(128, QUARTER)
+            block = gat[k][q].astype(F32).reshape(rows, QUARTER).astype(BF16)
             gate_pre = gate_pre + dot(block, gw[q * QUARTER : (q + 1) * QUARTER, :])
             up_pre = up_pre + dot(block, uw[q * QUARTER : (q + 1) * QUARTER, :])
         units = pl.ds(pl.multiple_of(y * HID, HID), HID)
-        hid[k, :, units] = (jax.nn.silu(gate_pre) * up_pre).astype(BF16)
+        hid[k][:, units] = (jax.nn.silu(gate_pre) * up_pre).astype(BF16)
         copies = []
         for d in (2, 1, 3):
             copies.append(
                 pltpu.make_async_remote_copy(
-                    hid.at[k, :, units], hid.at[k, :, units], H_SENT, hr_sem.at[k],
+                    hid[k].at[:, units], hid[k].at[:, units], H_SENT, hr_sem.at[k],
                     device_id=at(z, x, c, turn(y, d, NY)), device_id_type=MESH,
                 )
             )
@@ -306,8 +312,8 @@
         h_copies[k] = copies
 
     def down_chunk(k):
-        landed(hid.at[k, :, 0 : (NY - 1) * HID], hr_sem.at[k])
-        send[k] = dot(hid[k], dw[...]).astype(BF16).reshape(NC, NX, 16, QUARTER)
+        landed(hid[k].at[:, 0 : (NY - 1) * HID], hr_sem.at[k])
+        send[k][...] = dot(hid[k][...], dw[...]).reshape(send[k].shape).astype(BF16)
         copies = []
         for dx in (2, 1, 3, 0):
             for dc in range(NC):
@@ -315,7 +321,7 @@
                     to_x, to_c = turn(x, dx, NX), c if dc == 0 else 1 - c
                     copies.append(
                         pltpu.make_async_remote_copy(
-                            send.at[k, to_c, to_x], recv.at[k, dc * NX + dx - 1], R_SENT, rr_sem.at[k],
+                            send[k].at[to_c, to_x], recv[k].at[dc * NX + dx - 1], R_SENT, rr_sem.at[k],
                             device_id=at(z, to_x, to_c, y), device_id_type=MESH,
                         )
                     )
@@ -325,17 +331,18 @@
     b_copies = {}
 
     def home_chunk(k):
-        landed(recv.at[k], rr_sem.at[k])
-        total = send[k, c, x].astype(F32)
+        landed(recv[k], rr_sem.at[k])
+        total = send[k][c, x].astype(F32)
         for i in range(NC * NX - 1):
-            total = total + recv[k, i].astype(F32)
-        sum32[...] = total
-        for i in range(HALF):
-            back[k, i] = sum32[2 * i : 2 * i + 2, :].astype(BF16)
-        for i in range(HALF):
-            home = k * HALF + i
+            total = total + recv[k][i].astype(F32)
+        low, high = CHUNKS[k]
+        sum32[0 : 2 * (high - low), :] = total
+        for i in range(high - low):
+            back[k][i] = sum32[2 * i : 2 * i + 2, :].astype(BF16)
+        for i in range(high - low):
+            home = low + i
             b_copies[home] = pltpu.make_async_remote_copy(
-                back.at[k, i], zout.at[z], B_SENT, br_sem,
+                back[k].at[i], zout.at[z], B_SENT, br_sem,
                 device_id=at(home, x, c, y), device_id_type=MESH,
             )
 
@@ -345,24 +352,31 @@
 
             @pl.when(z == home)
             def _():
-                pltpu.make_async_copy(back.at[k, i], zout.at[z], br_sem).start()
+                pltpu.make_async_copy(back[k].at[i], zout.at[z], br_sem).start()
 
     take_chunk(0)
     gather_at_once(0)
     take_chunk(1)
     gather_along_y(1)
+    take_chunk(2)
+    gather_along_y(2)
     spread_chunk(0, (0, 1, 3, 2))
     gather_along_x(1)
+    gather_along_x(2)
     loads[17].wait()
     loads[18].wait()
     up_chunk(0)
+    spread_chunk(1, (1, 3, 2))
     loads[19].wait()
     down_chunk(0)
-    spread_chunk(1, (1, 3, 2))
+    spread_chunk(2, (1, 3, 2))
     up_chunk(1)
+    up_chunk(2)
     home_chunk(0)
     down_chunk(1)
+    down_chunk(2)
     home_chunk(1)
+    home_chunk(2)
 
     back_row = iota((2 * NZ, QUARTER), 0)
     _, scales = table(back_row // 4, back_row % 2, (2 * NZ, QUARTER))
@@ -381,7 +395,7 @@
         def _():
             copy.wait_send()
 
-    for copy in gathers + forwards + h_copies[0] + h_copies[1] + r_copies[0] + r_copies[1]:
+    for copy in gathers + forwards + sum(h_copies.values(), []) + sum(r_copies.values(), []):
         copy.wait_send()
 
 
@@ -419,19 +433,23 @@
         pltpu.VMEM((16, QUARTER), F32),
         pltpu.VMEM((8, 2, QUARTER), BF16),
         pltpu.VMEM((NZ, 2, QUARTER), BF16),
-        pltpu.VMEM((2, NY, NC, NX, 16, QUARTER), BF16),
-        pltpu.VMEM((2, 128, NY * HID), BF16),
-        pltpu.VMEM((2, NC, NX, 16, QUARTER), BF16),
-        pltpu.VMEM((2, NC * NX - 1, 16, QUARTER), BF16),
         pltpu.VMEM((16, QUARTER), F32),
-        pltpu.VMEM((2, 8, 2, QUARTER), BF16),
         pltpu.VMEM((NZ, 2, QUARTER), BF16),
         pltpu.VMEM((2 * NZ, QUARTER), F32),
         dma((9,)), dma((7,)),
-        dma, dma((2,)), dma((2, NX)), dma((2,)), dma((2,)), dma((2,)), dma,
+        dma, dma((3,)), dma((3, NX)), dma((3,)), dma((3,)), dma((3,)), dma,
         pltpu.SemaphoreType.REGULAR,
         pltpu.SemaphoreType.REGULAR,
     ]
+    for low, high in CHUNKS:
+        block = 2 * (high - low)
+        scratch += [
+            pltpu.VMEM((NY, NC, NX, block, QUARTER), BF16),
+            pltpu.VMEM((NC * NX * block, NY * HID), BF16),
+            pltpu.VMEM((NC, NX, block, QUARTER), BF16),
+            pltpu.VMEM((NC * NX - 1, block, QUARTER), BF16),
+            pltpu.VMEM((high - low, 2, QUARTER), BF16),
+        ]
     anywhere = pl.BlockSpec(memory_space=pl.ANY)
     near = pl.BlockSpec(memory_space=pltpu.VMEM)
     results = pl.pallas_call(

time: 47.3 us -> 46.6 us (0.985)
  Pallas kernels: 46.4 us -> 45.7 us
    pallas_call x1, Pallas kernels: 45.8 us -> 45.1 us  [shards(): pl.pallas_call(kernel, out_shape=tuple((pltpu.VMEM(*shape) for shape in s...]
where the time goes in v5:
time: 46.6 us; the launch traced here: 46.4 us
  Pallas kernels  45.7 us (98%)
  between operations  0.65 us (1%)
    pallas_call x1, Pallas kernels, shards(): pl.pallas_call(kernel, out_shape=tuple((pltpu.VMEM(*shape) for shape in s...  45.1 us

profile of v5, /device:TPU:1, one launch (start us, length us, event | category | flops | bytes accessed | tf_op | source)
XLA Modules:
  0.0 46.4 jit_solution(6260243952405316319)
XLA Ops:
  0.6 45.1 %shard_map.211 = (bf16[4,512]{1,0:T(4,128)(2,1)S(1)}, f32[4,16,64]{2,1,0:T(8,128)S(1)}, f32[4,16,64]{2,1,0:T(8,128)S(1)}) custom-call(bf16[4,2048]{1,0:T(4,128)(2,1)} %refs_0_.1, bf16[16,128]{1,0:T(8,128)(2,1)} %bitcast.9, bf16[2048,256]{1,0:T(8,128)(2,1)} %refs_2_.1, f32[16,64]{1,0:T(8,128)} %refs_3_.1, f32[16,64]{1,0:T(8,128)} %refs_4_.1, f32[16]{0:T(128)} %refs_5_.1, ...), custom_call_target="tpu_custom_call" | custom-call | tf_op jit(solution)/shard_map/pallas_call | solution.py:455
  45.7 0.7 %shard_map.212 = (bf16[4,512]{1,0:T(4,128)(2,1)}, f32[4,16,64]{2,1,0:T(8,128)}, f32[4,16,64]{2,1,0:T(8,128)}) custom-call(bf16[4,512]{1,0:T(4,128)(2,1)S(1)} %get-tuple-element.6.refs_0_, f32[4,16,64]{2,1,0:T(8,128)S(1)} %get-tuple-element.7.refs_1_, f32[4,16,64]{2,1,0:T(8,128)S(1)} %get-tuple-element.8.refs_2_), custom_call_target="tpu_custom_call" | custom-call | tf_op jit(solution)/shard_map/pallas_call | solution.py:465

commit v6 on v5

--- a/solution.py
+++ b/solution.py
@@ -78,6 +78,20 @@
         pltpu.make_async_remote_copy(
             ref, ref, D_SENT, sem, device_id=at(z, x, 1 - c, y), device_id_type=MESH
         ).wait_recv()
+
+    sent_by_all, sent_by, sent_home = [], ([], []), []
+
+    def send_away(source, target, send_sem, recv_sem, device, sent_list, alike):
+        pltpu.make_async_remote_copy(
+            source, target, send_sem, recv_sem, device_id=device, device_id_type=MESH
+        ).start()
+        sent_list.append((alike, send_sem))
+
+    def left(alike, sem):
+        ref = alike[0].at[alike[1]]
+        pltpu.make_async_remote_copy(
+            ref, ref, sem, dr_sem, device_id=at(z, x, 1 - c, y), device_id_type=MESH
+        ).wait_send()
 
     barrier = pltpu.get_barrier_semaphore()
 
@@ -233,150 +247,140 @@
     def _():
         pl.semaphore_wait(far_sem, 1)
 
-    z_copies = []
     for d in FAR_FIRST:
         to = turn(z, d, NZ)
-        z_copies.append(
-            pltpu.make_async_remote_copy(
-                pick.at[to // 2], zin.at[z], Z_SENT, zr_sem.at[chunk_of(z)],
-                device_id=at(to, x, c, y), device_id_type=MESH,
-            )
-        )
-        z_copies[-1].start()
-    pltpu.make_async_copy(pick.at[z // 2], zin.at[z], zr_sem.at[chunk_of(z)]).start()
-
-    gathers, forwards = [], []
+        send_away(pick.at[to // 2], zin.at[z, c], Z_SENT, zr_sem.at[chunk_of(z)], at(to, x, 1, y), sent_by_all, (pick, 0))
+    own_slots = (pick.at[z // 2], zin.at[z, c])
+
+    @pl.when(c == 1)
+    def _():
+        pltpu.make_async_copy(*own_slots, zr_sem.at[chunk_of(z)]).start()
+
+    @pl.when(c == 0)
+    def _():
+        send_away(*own_slots, Z_SENT, zr_sem.at[chunk_of(z)], at(z, x, 1, y), sent_by[0], (pick, 0))
 
     def take_chunk(k):
         low, high = CHUNKS[k]
+        block = 2 * (high - low)
         landed(zin.at[low:high], zr_sem.at[k])
-        for i in range(high - low):
-            sum32[2 * i : 2 * i + 2, :] = zin[low + i].astype(F32)
-        gat[k][y, c, x] = sum32[0 : 2 * (high - low), :].astype(BF16)
-
-    def pass_on(slots, k, dx, dy):
-        copy = pltpu.make_async_remote_copy(
-            slots, slots, G_SENT, gr_sem.at[k, dx],
-            device_id=at(z, turn(x, dx, NX), c, turn(y, dy, NY)), device_id_type=MESH,
-        )
-        copy.start()
-        gathers.append(copy)
+        for core in range(NC):
+            for i in range(high - low):
+                row = core * block + 2 * i
+                sum32[row : row + 2, :] = zin[low + i, core].astype(F32)
+        gat[k][y, x] = sum32[0 : 2 * block, :].astype(BF16)
+
+    def pass_on(slots, alike, k, dx, dy):
+        to = at(z, turn(x, dx, NX), 1, turn(y, dy, NY))
+        send_away(slots, slots, G_SENT, gr_sem.at[k, dx], to, sent_by[1], alike)
 
     def gather_at_once(k):
         for dx, dy in reversed(PLANE):
             if dx or dy:
-                pass_on(gat[k].at[y, c, x], k, dx, dy)
+                pass_on(gat[k].at[y, x], (gat[k], (0, 0)), k, dx, dy)
 
     def gather_along_y(k):
         for dy in (2, 1, 3):
-            pass_on(gat[k].at[y, c, x], k, 0, dy)
+            pass_on(gat[k].at[y, x], (gat[k], (0, 0)), k, 0, dy)
 
     def gather_along_x(k):
         spread_chunk(k, (0,))
         for dx in (2, 1, 3):
-            pass_on(gat[k].at[:, c, x], k, dx, 0)
-
-    h_copies, r_copies = {}, {}
+            pass_on(gat[k].at[:, x], (gat[k], (slice(None), 0)), k, dx, 0)
 
     def spread_chunk(k, distances):
         for dx in distances:
             rows_x = turn(x, NX - dx, NX)
-            landed(gat[k].at[(0 if dx else 1) : NY, c, rows_x], gr_sem.at[k, dx])
-            slots = gat[k].at[:, c, rows_x]
-            copy = pltpu.make_async_remote_copy(
-                slots, slots, F_SENT, fr_sem.at[k], device_id=at(z, x, 1 - c, y), device_id_type=MESH
-            )
-            copy.start()
-            forwards.append(copy)
+            landed(gat[k].at[(0 if dx else 1) : NY, rows_x], gr_sem.at[k, dx])
+            slots = gat[k].at[:, rows_x]
+            send_away(slots, slots, F_SENT, fr_sem.at[k], at(z, x, 0, y), sent_by[1], (gat[k], (slice(None), 0)))
 
     def up_chunk(k):
-        landed(gat[k].at[:, 1 - c], fr_sem.at[k])
+        @pl.when(c == 0)
+        def _():
+            landed(gat[k], fr_sem.at[k])
+
         rows = hid[k].shape[0]
         gate_pre = jnp.zeros((rows, HID), F32)
         up_pre = jnp.zeros((rows, HID), F32)
         for q in range(NY):
-            block = gat[k][q].astype(F32).reshape(rows, QUARTER).astype(BF16)
+            block = gat[k][q].reshape(rows, QUARTER)
             gate_pre = gate_pre + dot(block, gw[q * QUARTER : (q + 1) * QUARTER, :])
             up_pre = up_pre + dot(block, uw[q * QUARTER : (q + 1) * QUARTER, :])
         units = pl.ds(pl.multiple_of(y * HID, HID), HID)
         hid[k][:, units] = (jax.nn.silu(gate_pre) * up_pre).astype(BF16)
-        copies = []
+        own_units = hid[k].at[:, units]
         for d in (2, 1, 3):
-            copies.append(
-                pltpu.make_async_remote_copy(
-                    hid[k].at[:, units], hid[k].at[:, units], H_SENT, hr_sem.at[k],
-                    device_id=at(z, x, c, turn(y, d, NY)), device_id_type=MESH,
-                )
-            )
-            copies[-1].start()
-        h_copies[k] = copies
+            to = at(z, x, c, turn(y, d, NY))
+            send_away(own_units, own_units, H_SENT, hr_sem.at[k], to, sent_by_all, (hid[k], (slice(None), slice(0, HID))))
 
     def down_chunk(k):
         landed(hid[k].at[:, 0 : (NY - 1) * HID], hr_sem.at[k])
-        send[k][...] = dot(hid[k][...], dw[...]).reshape(send[k].shape).astype(BF16)
-        copies = []
-        for dx in (2, 1, 3, 0):
-            for dc in range(NC):
-                if dx or dc:
-                    to_x, to_c = turn(x, dx, NX), c if dc == 0 else 1 - c
-                    copies.append(
-                        pltpu.make_async_remote_copy(
-                            send[k].at[to_c, to_x], recv[k].at[dc * NX + dx - 1], R_SENT, rr_sem.at[k],
-                            device_id=at(z, to_x, to_c, y), device_id_type=MESH,
-                        )
-                    )
-                    copies[-1].start()
-        r_copies[k] = copies
-
-    b_copies = {}
+        send[k][...] = dot(hid[k][...], dw[...]).astype(BF16).reshape(send[k].shape)
+        for dx in (2, 1, 3):
+            to = turn(x, dx, NX)
+            slot = recv[k].at[2 * dx - 1 + c]
+            send_away(send[k].at[to], slot, R_SENT, rr_sem.at[k], at(z, to, 1, y), sent_by_all, (send[k], 0))
+
+        @pl.when(c == 0)
+        def _():
+            home = at(z, x, 1, y)
+            send_away(send[k].at[x], recv[k].at[0], R_SENT, rr_sem.at[k], home, sent_by[0], (send[k], 0))
 
     def home_chunk(k):
         landed(recv[k], rr_sem.at[k])
-        total = send[k][c, x].astype(F32)
+        total = send[k][x].astype(F32)
         for i in range(NC * NX - 1):
             total = total + recv[k][i].astype(F32)
         low, high = CHUNKS[k]
-        sum32[0 : 2 * (high - low), :] = total
-        for i in range(high - low):
-            back[k][i] = sum32[2 * i : 2 * i + 2, :].astype(BF16)
+        block = 2 * (high - low)
+        sum32[0 : 2 * block, :] = total
+        for core in range(NC):
+            for i in range(high - low):
+                row = core * block + 2 * i
+                back[k][i, core] = sum32[row : row + 2, :].astype(BF16)
         for i in range(high - low):
             home = low + i
-            b_copies[home] = pltpu.make_async_remote_copy(
-                back[k].at[i], zout.at[z], B_SENT, br_sem,
-                device_id=at(home, x, c, y), device_id_type=MESH,
-            )
+            slots = back[k].at[i, 0]
+            send_away(slots, zout.at[z], B_SENT, br_sem, at(home, x, 0, y), sent_by[1], (pick, 0))
 
             @pl.when(z != home)
             def _():
-                b_copies[home].start()
+                slots = back[k].at[i, 1]
+                send_away(slots, zout.at[z], B_SENT, br_sem, at(home, x, 1, y), sent_home, (pick, 0))
 
             @pl.when(z == home)
             def _():
-                pltpu.make_async_copy(back[k].at[i], zout.at[z], br_sem).start()
-
-    take_chunk(0)
-    gather_at_once(0)
-    take_chunk(1)
-    gather_along_y(1)
-    take_chunk(2)
-    gather_along_y(2)
-    spread_chunk(0, (0, 1, 3, 2))
-    gather_along_x(1)
-    gather_along_x(2)
+                pltpu.make_async_copy(back[k].at[i, 1], zout.at[z], br_sem).start()
+
+    on_core_1 = pl.when(c == 1)
+
+    @on_core_1
+    def _():
+        take_chunk(0)
+        gather_at_once(0)
+        take_chunk(1)
+        gather_along_y(1)
+        take_chunk(2)
+        gather_along_y(2)
+        spread_chunk(0, (0, 1, 3, 2))
+        gather_along_x(1)
+        gather_along_x(2)
+
     loads[17].wait()
     loads[18].wait()
     up_chunk(0)
-    spread_chunk(1, (1, 3, 2))
+    on_core_1(lambda: spread_chunk(1, (1, 3, 2)))
     loads[19].wait()
     down_chunk(0)
-    spread_chunk(2, (1, 3, 2))
+    on_core_1(lambda: spread_chunk(2, (1, 3, 2)))
     up_chunk(1)
     up_chunk(2)
-    home_chunk(0)
+    on_core_1(lambda: home_chunk(0))
     down_chunk(1)
     down_chunk(2)
-    home_chunk(1)
-    home_chunk(2)
+    on_core_1(lambda: home_chunk(1))
+    on_core_1(lambda: home_chunk(2))
 
     back_row = iota((2 * NZ, QUARTER), 0)
     _, scales = table(back_row // 4, back_row % 2, (2 * NZ, QUARTER))
@@ -387,16 +391,22 @@
     routed = [jnp.sum(scales[s] * pieces, axis=0, keepdims=True) for s in range(SEQ)]
     mixed_o[...] = (hid32[:, lanes] + jnp.concatenate(routed, axis=0)).astype(BF16)
 
-    for copy in delta_copies + z_copies:
+    for copy in delta_copies:
         copy.wait_send()
-    for home, copy in b_copies.items():
-
-        @pl.when(z != home)
+    for copy in sent_by_all:
+        left(*copy)
+    for core in range(NC):
+
+        @pl.when(c == core)
         def _():
-            copy.wait_send()
-
-    for copy in gathers + forwards + sum(h_copies.values(), []) + sum(r_copies.values(), []):
-        copy.wait_send()
+            for copy in sent_by[core]:
+                left(*copy)
+
+    for home, copy in enumerate(sent_home):
+
+        @pl.when((c == 1) & (z != home))
+        def _():
+            left(*copy)
 
 
 def store_kernel(*refs):
@@ -432,8 +442,8 @@
         pltpu.VMEM((SEQ, WIDTH), F32),
         pltpu.VMEM((16, QUARTER), F32),
         pltpu.VMEM((8, 2, QUARTER), BF16),
-        pltpu.VMEM((NZ, 2, QUARTER), BF16),
-        pltpu.VMEM((16, QUARTER), F32),
+        pltpu.VMEM((NZ, NC, 2, QUARTER), BF16),
+        pltpu.VMEM((32, QUARTER), F32),
         pltpu.VMEM((NZ, 2, QUARTER), BF16),
         pltpu.VMEM((2 * NZ, QUARTER), F32),
         dma((9,)), dma((7,)),
@@ -442,13 +452,13 @@
         pltpu.SemaphoreType.REGULAR,
     ]
     for low, high in CHUNKS:
-        block = 2 * (high - low)
+        block = 2 * NC * (high - low)
         scratch += [
-            pltpu.VMEM((NY, NC, NX, block, QUARTER), BF16),
-            pltpu.VMEM((NC * NX * block, NY * HID), BF16),
-            pltpu.VMEM((NC, NX, block, QUARTER), BF16),
+            pltpu.VMEM((NY, NX, block, QUARTER), BF16),
+            pltpu.VMEM((NX * block, NY * HID), BF16),
+            pltpu.VMEM((NX, block, QUARTER), BF16),
             pltpu.VMEM((NC * NX - 1, block, QUARTER), BF16),
-            pltpu.VMEM((high - low, 2, QUARTER), BF16),
+            pltpu.VMEM((high - low, NC, 2, QUARTER), BF16),
         ]
     anywhere = pl.BlockSpec(memory_space=pl.ANY)
     near = pl.BlockSpec(memory_space=pltpu.VMEM)

time: 46.6 us -> 46.4 us (level)
  no operation moved by 1% of the time
where the time goes in v6:
time: 46.4 us; the launch traced here: 46.2 us
  Pallas kernels  45.6 us (98%)
  between operations  0.65 us (1%)
    pallas_call x1, Pallas kernels, shards(): pl.pallas_call(kernel, out_shape=tuple((pltpu.VMEM(*shape) for shape in s...  44.9 us

profile of v6, /device:TPU:1, one launch (start us, length us, event | category | flops | bytes accessed | tf_op | source)
XLA Modules:
  0.0 46.2 jit_solution(5334356820476137022)
XLA Ops:
  0.6 44.9 %shard_map.211 = (bf16[4,512]{1,0:T(4,128)(2,1)S(1)}, f32[4,16,64]{2,1,0:T(8,128)S(1)}, f32[4,16,64]{2,1,0:T(8,128)S(1)}) custom-call(bf16[4,2048]{1,0:T(4,128)(2,1)} %refs_0_.1, bf16[16,128]{1,0:T(8,128)(2,1)} %bitcast.9, bf16[2048,256]{1,0:T(8,128)(2,1)} %refs_2_.1, f32[16,64]{1,0:T(8,128)} %refs_3_.1, f32[16,64]{1,0:T(8,128)} %refs_4_.1, f32[16]{0:T(128)} %refs_5_.1, ...), custom_call_target="tpu_custom_call" | custom-call | tf_op jit(solution)/shard_map/pallas_call | solution.py:465
  45.6 0.7 %shard_map.212 = (bf16[4,512]{1,0:T(4,128)(2,1)}, f32[4,16,64]{2,1,0:T(8,128)}, f32[4,16,64]{2,1,0:T(8,128)}) custom-call(bf16[4,512]{1,0:T(4,128)(2,1)S(1)} %get-tuple-element.6.refs_0_, f32[4,16,64]{2,1,0:T(8,128)S(1)} %get-tuple-element.7.refs_1_, f32[4,16,64]{2,1,0:T(8,128)S(1)} %get-tuple-element.8.refs_2_), custom_call_target="tpu_custom_call" | custom-call | tf_op jit(solution)/shard_map/pallas_call | solution.py:475

commit v7 on v6

--- a/solution.py
+++ b/solution.py
@@ -13,6 +13,7 @@
 GROUPS, STATE, CHANNELS = 16, 64, 256
 HID = 128
 CHUNKS = ((0, 4), (4, 8), (8, 16))
+SUMS = (1, 1, 0)
 FAR_FIRST = (8, 7, 9, 6, 10, 5, 11, 4, 12, 3, 13, 2, 14, 1, 15)
 VMEM_LIMIT = 67043328 - 72 * 1024
 LOAD_GROUP = (0, 0, 1, 2, 2, 2, 2, 2, 4, 4, 4, 3, 3, 5, 6, 6, 6, 7, 7, 8)
@@ -98,8 +99,20 @@
     def enter(device):
         pl.semaphore_signal(barrier, inc=1, device_id=device, device_id_type=MESH)
 
-    for d in FAR_FIRST:
-        enter(at(turn(z, d, NZ), x, 1, y))
+    wide = pl.multiple_of((ep // 32) * 128, 128)
+    sources = list(hbm)
+    sources[15] = ids_h.at[:, pl.ds(wide, 128)]
+    loads = [
+        pltpu.make_async_copy(source, target, load.at[LOAD_GROUP[i]])
+        for i, (source, target) in enumerate(zip(sources, scratch[:20]))
+    ]
+    @pl.when(c == 1)
+    def _():
+        for d in FAR_FIRST:
+            enter(at(turn(z, d, NZ), x, 1, y))
+
+    for i in (0, 1, 2):
+        loads[i].start()
     for d in range(1, NY):
         enter(at(z, x, 0, turn(y, d, NY)))
     for dx, dy in PLANE:
@@ -107,16 +120,9 @@
             enter(at(z, turn(x, dx, NX), 1, turn(y, dy, NY)))
     enter(at(z, x, 1 - c, y))
     near_count = 2 * (NY - 1) + 1
-    far_count = 2 * (NZ - 1) + 2 * (NX * NY - 1) + 1
-
-    wide = pl.multiple_of((ep // 32) * 128, 128)
-    sources = list(hbm)
-    sources[15] = ids_h.at[:, pl.ds(wide, 128)]
-    loads = [
-        pltpu.make_async_copy(source, target, load.at[LOAD_GROUP[i]])
-        for i, (source, target) in enumerate(zip(sources, scratch[:20]))
-    ]
-    for i in (0, 1, 2, 3, 4, 5, 6, 7, 11, 12, 8, 9, 10, 13, 14, 15, 16, 17, 18, 19):
+    far_count = (NZ - 1) + 2 * (NX * NY - 1) + 1
+
+    for i in (3, 4, 5, 6, 7, 11, 12, 8, 9, 10, 13, 14, 15, 16, 17, 18, 19):
         loads[i].start()
 
     loads[0].wait()
@@ -320,12 +326,13 @@
         for dx in (2, 1, 3):
             to = turn(x, dx, NX)
             slot = recv[k].at[2 * dx - 1 + c]
-            send_away(send[k].at[to], slot, R_SENT, rr_sem.at[k], at(z, to, 1, y), sent_by_all, (send[k], 0))
-
-        @pl.when(c == 0)
+            send_away(send[k].at[to], slot, R_SENT, rr_sem.at[k], at(z, to, SUMS[k], y), sent_by_all, (send[k], 0))
+
+        @pl.when(c != SUMS[k])
         def _():
-            home = at(z, x, 1, y)
-            send_away(send[k].at[x], recv[k].at[0], R_SENT, rr_sem.at[k], home, sent_by[0], (send[k], 0))
+            home = at(z, x, SUMS[k], y)
+            kept = sent_by[1 - SUMS[k]]
+            send_away(send[k].at[x], recv[k].at[0], R_SENT, rr_sem.at[k], home, kept, (send[k], 0))
 
     def home_chunk(k):
         landed(recv[k], rr_sem.at[k])
@@ -341,17 +348,17 @@
                 back[k][i, core] = sum32[row : row + 2, :].astype(BF16)
         for i in range(high - low):
             home = low + i
-            slots = back[k].at[i, 0]
-            send_away(slots, zout.at[z], B_SENT, br_sem, at(home, x, 0, y), sent_by[1], (pick, 0))
+            slots, other = back[k].at[i, 1 - SUMS[k]], at(home, x, 1 - SUMS[k], y)
+            send_away(slots, zout.at[z], B_SENT, br_sem, other, sent_by[SUMS[k]], (pick, 0))
 
             @pl.when(z != home)
             def _():
-                slots = back[k].at[i, 1]
-                send_away(slots, zout.at[z], B_SENT, br_sem, at(home, x, 1, y), sent_home, (pick, 0))
+                slots, same = back[k].at[i, SUMS[k]], at(home, x, SUMS[k], y)
+                send_away(slots, zout.at[z], B_SENT, br_sem, same, sent_home, (pick, 0))
 
             @pl.when(z == home)
             def _():
-                pltpu.make_async_copy(back[k].at[i, 1], zout.at[z], br_sem).start()
+                pltpu.make_async_copy(back[k].at[i, SUMS[k]], zout.at[z], br_sem).start()
 
     on_core_1 = pl.when(c == 1)
 
@@ -380,7 +387,7 @@
     down_chunk(1)
     down_chunk(2)
     on_core_1(lambda: home_chunk(1))
-    on_core_1(lambda: home_chunk(2))
+    pl.when(c == SUMS[2])(lambda: home_chunk(2))
 
     back_row = iota((2 * NZ, QUARTER), 0)
     _, scales = table(back_row // 4, back_row % 2, (2 * NZ, QUARTER))
@@ -404,7 +411,7 @@
 
     for home, copy in enumerate(sent_home):
 
-        @pl.when((c == 1) & (z != home))
+        @pl.when((c == SUMS[0 if home < 4 else 1 if home < 8 else 2]) & (z != home))
         def _():
             left(*copy)
 

time: 46.4 us -> 45.1 us (0.972); the launches traced: 46.2 us -> 44.4 us
  Pallas kernels: 45.6 us -> 43.7 us
    pallas_call x1, Pallas kernels: 44.9 us -> 43.1 us  [shards(): pl.pallas_call(kernel, out_shape=tuple((pltpu.VMEM(*shape) for shape in s...]
where the time goes in v7:
time: 45.1 us; the launch traced here: 44.4 us
  Pallas kernels  43.7 us (97%)
  between operations  0.65 us (1%)
    pallas_call x1, Pallas kernels, shards(): pl.pallas_call(kernel, out_shape=tuple((pltpu.VMEM(*shape) for shape in s...  43.1 us

profile of v7, /device:TPU:1, one launch (start us, length us, event | category | flops | bytes accessed | tf_op | source)
XLA Modules:
  0.0 44.4 jit_solution(15525482278700358367)
XLA Ops:
  0.6 43.1 %shard_map.211 = (bf16[4,512]{1,0:T(4,128)(2,1)S(1)}, f32[4,16,64]{2,1,0:T(8,128)S(1)}, f32[4,16,64]{2,1,0:T(8,128)S(1)}) custom-call(bf16[4,2048]{1,0:T(4,128)(2,1)} %refs_0_.1, bf16[16,128]{1,0:T(8,128)(2,1)} %bitcast.9, bf16[2048,256]{1,0:T(8,128)(2,1)} %refs_2_.1, f32[16,64]{1,0:T(8,128)} %refs_3_.1, f32[16,64]{1,0:T(8,128)} %refs_4_.1, f32[16]{0:T(128)} %refs_5_.1, ...), custom_call_target="tpu_custom_call" | custom-call | tf_op jit(solution)/shard_map/pallas_call | solution.py:472
  43.7 0.7 %shard_map.212 = (bf16[4,512]{1,0:T(4,128)(2,1)}, f32[4,16,64]{2,1,0:T(8,128)}, f32[4,16,64]{2,1,0:T(8,128)}) custom-call(bf16[4,512]{1,0:T(4,128)(2,1)S(1)} %get-tuple-element.6.refs_0_, f32[4,16,64]{2,1,0:T(8,128)S(1)} %get-tuple-element.7.refs_1_, f32[4,16,64]{2,1,0:T(8,128)S(1)} %get-tuple-element.8.refs_2_), custom_call_target="tpu_custom_call" | custom-call | tf_op jit(solution)/shard_map/pallas_call | solution.py:482

commit v8 on v7

--- a/solution.py
+++ b/solution.py
@@ -12,8 +12,9 @@
 SEQ, WIDTH, QUARTER = 4, 2048, 512
 GROUPS, STATE, CHANNELS = 16, 64, 256
 HID = 128
-CHUNKS = ((0, 4), (4, 8), (8, 16))
-SUMS = (1, 1, 0)
+CHUNKS = ((0, 4), (4, 8), (8, 12), (12, 16))
+X_FIRST = 3
+SUMS = (1, 1, 1, 0)
 FAR_FIRST = (8, 7, 9, 6, 10, 5, 11, 4, 12, 3, 13, 2, 14, 1, 15)
 VMEM_LIMIT = 67043328 - 72 * 1024
 LOAD_GROUP = (0, 0, 1, 2, 2, 2, 2, 2, 4, 4, 4, 3, 3, 5, 6, 6, 6, 7, 7, 8)
@@ -70,7 +71,7 @@
         return (zz * 8 + xx * 2 + cc, yy)
 
     def chunk_of(home):
-        return lax.min(home // 4, 2)
+        return home // 4
 
     def turn(a, d, n):
         return lax.rem(a + d, n)
@@ -276,30 +277,37 @@
                 sum32[row : row + 2, :] = zin[low + i, core].astype(F32)
         gat[k][y, x] = sum32[0 : 2 * block, :].astype(BF16)
 
-    def pass_on(slots, alike, k, dx, dy):
+    def pass_on(slots, alike, k, sem, dx, dy):
         to = at(z, turn(x, dx, NX), 1, turn(y, dy, NY))
-        send_away(slots, slots, G_SENT, gr_sem.at[k, dx], to, sent_by[1], alike)
+        send_away(slots, slots, G_SENT, gr_sem.at[k, sem], to, sent_by[1], (gat[k], alike))
+
+    def line(k, distance):
+        if k == X_FIRST:
+            return gat[k].at[turn(y, NY - distance, NY), :]
+        return gat[k].at[:, turn(x, NX - distance, NX)]
 
     def gather_at_once(k):
         for dx, dy in reversed(PLANE):
             if dx or dy:
-                pass_on(gat[k].at[y, x], (gat[k], (0, 0)), k, dx, dy)
-
-    def gather_along_y(k):
-        for dy in (2, 1, 3):
-            pass_on(gat[k].at[y, x], (gat[k], (0, 0)), k, 0, dy)
-
-    def gather_along_x(k):
+                pass_on(gat[k].at[y, x], (0, 0), k, dx, dx, dy)
+
+    def gather_first(k):
+        for d in (2, 1, 3):
+            dx, dy = (d, 0) if k == X_FIRST else (0, d)
+            pass_on(gat[k].at[y, x], (0, 0), k, 0, dx, dy)
+
+    def gather_second(k):
         spread_chunk(k, (0,))
-        for dx in (2, 1, 3):
-            pass_on(gat[k].at[:, x], (gat[k], (slice(None), 0)), k, dx, 0)
+        for d in (2, 1, 3):
+            dx, dy = (0, d) if k == X_FIRST else (d, 0)
+            pass_on(line(k, 0), (slice(None), 0), k, d, dx, dy)
 
     def spread_chunk(k, distances):
-        for dx in distances:
-            rows_x = turn(x, NX - dx, NX)
-            landed(gat[k].at[(0 if dx else 1) : NY, rows_x], gr_sem.at[k, dx])
-            slots = gat[k].at[:, rows_x]
-            send_away(slots, slots, F_SENT, fr_sem.at[k], at(z, x, 0, y), sent_by[1], (gat[k], (slice(None), 0)))
+        for d in distances:
+            landed(gat[k].at[0, (0 if d else 1) : NX], gr_sem.at[k, d])
+            send_away(
+                line(k, d), line(k, d), F_SENT, fr_sem.at[k], at(z, x, 0, y), sent_by[1], (gat[k], (slice(None), 0))
+            )
 
     def up_chunk(k):
         @pl.when(c == 0)
@@ -366,28 +374,36 @@
     def _():
         take_chunk(0)
         gather_at_once(0)
-        take_chunk(1)
-        gather_along_y(1)
-        take_chunk(2)
-        gather_along_y(2)
+        for k in (1, 2, 3):
+            take_chunk(k)
+            gather_first(k)
         spread_chunk(0, (0, 1, 3, 2))
-        gather_along_x(1)
-        gather_along_x(2)
+        gather_second(1)
+        gather_second(2)
 
     loads[17].wait()
     loads[18].wait()
     up_chunk(0)
-    on_core_1(lambda: spread_chunk(1, (1, 3, 2)))
+
+    @on_core_1
+    def _():
+        gather_second(3)
+        spread_chunk(1, (1, 3, 2))
+
     loads[19].wait()
     down_chunk(0)
     on_core_1(lambda: spread_chunk(2, (1, 3, 2)))
     up_chunk(1)
     up_chunk(2)
+    on_core_1(lambda: spread_chunk(3, (1, 3, 2)))
+    up_chunk(3)
     on_core_1(lambda: home_chunk(0))
     down_chunk(1)
     down_chunk(2)
+    down_chunk(3)
     on_core_1(lambda: home_chunk(1))
-    pl.when(c == SUMS[2])(lambda: home_chunk(2))
+    on_core_1(lambda: home_chunk(2))
+    pl.when(c == SUMS[3])(lambda: home_chunk(3))
 
     back_row = iota((2 * NZ, QUARTER), 0)
     _, scales = table(back_row // 4, back_row % 2, (2 * NZ, QUARTER))
@@ -411,7 +427,7 @@
 
     for home, copy in enumerate(sent_home):
 
-        @pl.when((c == SUMS[0 if home < 4 else 1 if home < 8 else 2]) & (z != home))
+        @pl.when((c == SUMS[home // 4]) & (z != home))
         def _():
             left(*copy)
 
@@ -450,11 +466,11 @@
         pltpu.VMEM((16, QUARTER), F32),
         pltpu.VMEM((8, 2, QUARTER), BF16),
         pltpu.VMEM((NZ, NC, 2, QUARTER), BF16),
-        pltpu.VMEM((32, QUARTER), F32),
+        pltpu.VMEM((16, QUARTER), F32),
         pltpu.VMEM((NZ, 2, QUARTER), BF16),
         pltpu.VMEM((2 * NZ, QUARTER), F32),
         dma((9,)), dma((7,)),
-        dma, dma((3,)), dma((3, NX)), dma((3,)), dma((3,)), dma((3,)), dma,
+        dma, dma((4,)), dma((4, NX)), dma((4,)), dma((4,)), dma((4,)), dma,
         pltpu.SemaphoreType.REGULAR,
         pltpu.SemaphoreType.REGULAR,
     ]

time: 45.1 us -> 45 us (level); the launches traced: 44.4 us -> 44.8 us
  Pallas kernels: 43.7 us -> 44.2 us
    pallas_call x1, Pallas kernels: 43.1 us -> 43.5 us  [shards(): pl.pallas_call(kernel, out_shape=tuple((pltpu.VMEM(*shape) for shape in s...]
where the time goes in v8:
time: 45 us; the launch traced here: 44.8 us
  Pallas kernels  44.2 us (98%)
  between operations  0.65 us (1%)
    pallas_call x1, Pallas kernels, shards(): pl.pallas_call(kernel, out_shape=tuple((pltpu.VMEM(*shape) for shape in s...  43.5 us

profile of v8, /device:TPU:1, one launch (start us, length us, event | category | flops | bytes accessed | tf_op | source)
XLA Modules:
  0.0 44.8 jit_solution(10121709248398496297)
XLA Ops:
  0.6 43.5 %shard_map.211 = (bf16[4,512]{1,0:T(4,128)(2,1)S(1)}, f32[4,16,64]{2,1,0:T(8,128)S(1)}, f32[4,16,64]{2,1,0:T(8,128)S(1)}) custom-call(bf16[4,2048]{1,0:T(4,128)(2,1)} %refs_0_.1, bf16[16,128]{1,0:T(8,128)(2,1)} %bitcast.9, bf16[2048,256]{1,0:T(8,128)(2,1)} %refs_2_.1, f32[16,64]{1,0:T(8,128)} %refs_3_.1, f32[16,64]{1,0:T(8,128)} %refs_4_.1, f32[16]{0:T(128)} %refs_5_.1, ...), custom_call_target="tpu_custom_call" | custom-call | tf_op jit(solution)/shard_map/pallas_call | solution.py:488
  44.2 0.7 %shard_map.212 = (bf16[4,512]{1,0:T(4,128)(2,1)}, f32[4,16,64]{2,1,0:T(8,128)}, f32[4,16,64]{2,1,0:T(8,128)}) custom-call(bf16[4,512]{1,0:T(4,128)(2,1)S(1)} %get-tuple-element.6.refs_0_, f32[4,16,64]{2,1,0:T(8,128)S(1)} %get-tuple-element.7.refs_1_, f32[4,16,64]{2,1,0:T(8,128)S(1)} %get-tuple-element.8.refs_2_), custom_call_target="tpu_custom_call" | custom-call | tf_op jit(solution)/shard_map/pallas_call | solution.py:498

commit v9 on v8

--- a/solution.py
+++ b/solution.py
@@ -387,8 +387,8 @@
 
     @on_core_1
     def _():
+        spread_chunk(1, (1, 3, 2))
         gather_second(3)
-        spread_chunk(1, (1, 3, 2))
 
     loads[19].wait()
     down_chunk(0)

time: 45 us -> 44.6 us (level)
  no operation moved by 1% of the time
where the time goes in v9:
time: 44.6 us; the launch traced here: 44.4 us
  Pallas kernels  43.8 us (98%)
  between operations  0.65 us (1%)
    pallas_call x1, Pallas kernels, shards(): pl.pallas_call(kernel, out_shape=tuple((pltpu.VMEM(*shape) for shape in s...  43.1 us

profile of v9, /device:TPU:1, one launch (start us, length us, event | category | flops | bytes accessed | tf_op | source)
XLA Modules:
  0.0 44.4 jit_solution(6831378306275192455)
XLA Ops:
  0.6 43.1 %shard_map.211 = (bf16[4,512]{1,0:T(4,128)(2,1)S(1)}, f32[4,16,64]{2,1,0:T(8,128)S(1)}, f32[4,16,64]{2,1,0:T(8,128)S(1)}) custom-call(bf16[4,2048]{1,0:T(4,128)(2,1)} %refs_0_.1, bf16[16,128]{1,0:T(8,128)(2,1)} %bitcast.9, bf16[2048,256]{1,0:T(8,128)(2,1)} %refs_2_.1, f32[16,64]{1,0:T(8,128)} %refs_3_.1, f32[16,64]{1,0:T(8,128)} %refs_4_.1, f32[16]{0:T(128)} %refs_5_.1, ...), custom_call_target="tpu_custom_call" | custom-call | tf_op jit(solution)/shard_map/pallas_call | solution.py:488
  43.8 0.7 %shard_map.212 = (bf16[4,512]{1,0:T(4,128)(2,1)}, f32[4,16,64]{2,1,0:T(8,128)}, f32[4,16,64]{2,1,0:T(8,128)}) custom-call(bf16[4,512]{1,0:T(4,128)(2,1)S(1)} %get-tuple-element.6.refs_0_, f32[4,16,64]{2,1,0:T(8,128)S(1)} %get-tuple-element.7.refs_1_, f32[4,16,64]{2,1,0:T(8,128)S(1)} %get-tuple-element.8.refs_2_), custom_call_target="tpu_custom_call" | custom-call | tf_op jit(solution)/shard_map/pallas_call | solution.py:498

commit v10 on v9

--- a/solution.py
+++ b/solution.py
@@ -62,7 +62,7 @@
     sum32, zout, out32 = scratch[26:29]
     load, sent, dr_sem, zr_sem, gr_sem, fr_sem, hr_sem, rr_sem, br_sem, near_sem, far_sem = scratch[29:40]
     gat, hid, send, recv, back = (scratch[40 + i :: 5] for i in range(5))
-    D_SENT, Z_SENT, G_SENT, F_SENT, H_SENT, R_SENT, B_SENT = (sent.at[i] for i in range(7))
+    D_SENT = Z_SENT = G_SENT = F_SENT = H_SENT = R_SENT = B_SENT = sent
 
     ep, y = lax.axis_index("ep"), lax.axis_index("tp")
     z, x, c = ep // 8, (ep // 2) % NX, ep % 2
@@ -350,11 +350,10 @@
         low, high = CHUNKS[k]
         block = 2 * (high - low)
         sum32[0 : 2 * block, :] = total
-        for core in range(NC):
-            for i in range(high - low):
+        for i in range(high - low):
+            for core in range(NC):
                 row = core * block + 2 * i
                 back[k][i, core] = sum32[row : row + 2, :].astype(BF16)
-        for i in range(high - low):
             home = low + i
             slots, other = back[k].at[i, 1 - SUMS[k]], at(home, x, 1 - SUMS[k], y)
             send_away(slots, zout.at[z], B_SENT, br_sem, other, sent_by[SUMS[k]], (pick, 0))
@@ -469,7 +468,7 @@
         pltpu.VMEM((16, QUARTER), F32),
         pltpu.VMEM((NZ, 2, QUARTER), BF16),
         pltpu.VMEM((2 * NZ, QUARTER), F32),
-        dma((9,)), dma((7,)),
+        dma((9,)), dma,
         dma, dma((4,)), dma((4, NX)), dma((4,)), dma((4,)), dma((4,)), dma,
         pltpu.SemaphoreType.REGULAR,
         pltpu.SemaphoreType.REGULAR,

time: 44.6 us -> 44.5 us (level)
  no operation moved by 1% of the time
where the time goes in v10:
time: 44.5 us; the launch traced here: 44.4 us
  Pallas kernels  43.7 us (98%)
  between operations  0.65 us (1%)
    pallas_call x1, Pallas kernels, shards(): pl.pallas_call(kernel, out_shape=tuple((pltpu.VMEM(*shape) for shape in s...  43.1 us

profile of v10, /device:TPU:1, one launch (start us, length us, event | category | flops | bytes accessed | tf_op | source)
XLA Modules:
  0.0 44.4 jit_solution(1130055393494409186)
XLA Ops:
  0.6 43.1 %shard_map.211 = (bf16[4,512]{1,0:T(4,128)(2,1)S(1)}, f32[4,16,64]{2,1,0:T(8,128)S(1)}, f32[4,16,64]{2,1,0:T(8,128)S(1)}) custom-call(bf16[4,2048]{1,0:T(4,128)(2,1)} %refs_0_.1, bf16[16,128]{1,0:T(8,128)(2,1)} %bitcast.9, bf16[2048,256]{1,0:T(8,128)(2,1)} %refs_2_.1, f32[16,64]{1,0:T(8,128)} %refs_3_.1, f32[16,64]{1,0:T(8,128)} %refs_4_.1, f32[16]{0:T(128)} %refs_5_.1, ...), custom_call_target="tpu_custom_call" | custom-call | tf_op jit(solution)/shard_map/pallas_call | solution.py:487
  43.7 0.7 %shard_map.212 = (bf16[4,512]{1,0:T(4,128)(2,1)}, f32[4,16,64]{2,1,0:T(8,128)}, f32[4,16,64]{2,1,0:T(8,128)}) custom-call(bf16[4,512]{1,0:T(4,128)(2,1)S(1)} %get-tuple-element.6.refs_0_, f32[4,16,64]{2,1,0:T(8,128)S(1)} %get-tuple-element.7.refs_1_, f32[4,16,64]{2,1,0:T(8,128)S(1)} %get-tuple-element.8.refs_2_), custom_call_target="tpu_custom_call" | custom-call | tf_op jit(solution)/shard_map/pallas_call | solution.py:497
